TPU v7x, 128 devices: a whole 4x4x4 slice. The times are simulated.
128 devices in a mesh: rep: 2 (over z_hi), fs: 32 (over z_lo, y, x), tp: 2 (over core).
Axes of the slice: x: 4, y: 4, z: 4 (z_hi: 2, z_lo: 2; z = z_hi * 2 + z_lo), core: 2. Of those that a mesh axis runs over, the one named last changes fastest.
Arguments:
- tokens: bfloat16 [64, 256, 1024], P(('rep', 'fs'), None, 'tp'), may hold values from -6 to 6
- pre_gain: float32 [1024], replicated, may hold values from 0.1 to 1.9
- first_gate: bfloat16 [1024, 2560], P('fs', 'tp'), may hold values from -0.1875 to 0.1875
- first_up: bfloat16 [1024, 2560], P('fs', 'tp'), may hold values from -0.1875 to 0.1875
- first_down: bfloat16 [2560, 1024], P('tp', 'fs'), may hold values from -0.125 to 0.125
- mix_gain: float32 [1024], P('tp'), may hold values from 0.1 to 1.9
- pool_weight: bfloat16 [4, 256, 256], P('tp', None, 'fs'), may hold values from -0.375 to 0.375
- pool_scale: float32 [1024], P('tp'), may hold values from 0.1 to 1.9
- post_gain: float32 [1024], replicated, may hold values from 0.1 to 1.9
- second_gate: bfloat16 [1024, 2560], P('fs', 'tp'), may hold values from -0.1875 to 0.1875
- second_up: bfloat16 [1024, 2560], P('fs', 'tp'), may hold values from -0.1875 to 0.1875
- second_down: bfloat16 [2560, 1024], P('tp', 'fs'), may hold values from -0.125 to 0.125
Outputs:
- layer_out: bfloat16 [64, 256, 1024], P(('rep', 'fs'), None, 'tp')
All inputs are finite; a program needn't handle non-finite values.
Results may differ from a plain program's by a relative error of at most 0.015.
Values may be sent and summed in bfloat16 or wider, within the bound.
A program may use at most 64 MiB of HBM per device.

v0:
```python
import jax
import jax.numpy as jnp
from jax import lax
from jax.sharding import PartitionSpec as P

D = 1024
GROUPS = 4


epsilon = 1e-06


def taken_in(shard, axis, dim, take_in, carry):
    whole = jax.tree.map(lambda part: lax.all_gather(part, axis, axis=dim, tiled=True), shard)
    return take_in(carry, whole, jnp.int32(0))


def over_all(shard, axis, dim, block):
    whole = lax.all_gather(shard, axis, axis=dim, tiled=True)
    return block(whole, jnp.int32(0))


def normalize(values, gain_vec):
    floats = values.astype(jnp.float32)
    scaled = floats * lax.rsqrt(jnp.mean(floats * floats, axis=-1, keepdims=True) + epsilon)
    return (scaled * gain_vec.astype(jnp.float32)).astype(jnp.bfloat16)


def half_step(local_part, gain_vec, gate_w, up_w, down_w):
    gathered = lax.all_gather(local_part, "tp", axis=2, tiled=True)
    seq_count, seq_length, full_width = gathered.shape
    normed = normalize(gathered.reshape(seq_count * seq_length, full_width), gain_vec)
    zero_init = jnp.zeros((normed.shape[0], gate_w.shape[1]), jnp.float32)

    def add_rows(running, block_rows, offset):
        columns = lax.dynamic_slice_in_dim(normed, offset, block_rows.shape[0], 1)
        return running + jnp.dot(columns, block_rows, preferred_element_type=jnp.float32)

    gate_sum = taken_in(gate_w, "fs", 0, add_rows, zero_init)
    up_sum = taken_in(up_w, "fs", 0, add_rows, zero_init)
    hidden = (jax.nn.silu(gate_sum) * up_sum).astype(jnp.bfloat16)

    def project(block_cols, offset):
        return jnp.dot(hidden, block_cols, preferred_element_type=jnp.float32)

    partial_value = over_all(down_w, "fs", 1, project)
    own_part = lax.psum_scatter(
        partial_value.astype(jnp.bfloat16), "tp", scatter_dimension=1, tiled=True
    ).astype(jnp.float32)
    return own_part.reshape(seq_count, seq_length, own_part.shape[1])


def trailing(grouped, windows, widest):
    seq_length = grouped.shape[1]
    running = jnp.zeros_like(grouped)
    for back_step in range(widest):
        moved = jnp.pad(grouped, ((0, 0), (back_step, 0), (0, 0), (0, 0)))[:, :seq_length]
        running = running + jnp.where(back_step < windows[None, None, :, None], moved, 0.0)
    positions = jnp.arange(seq_length, dtype=jnp.int32)
    counts = jnp.minimum(positions[:, None] + 1, windows[None, :]).astype(jnp.float32)
    return running / counts[None, :, :, None]


def pool_mix(local_part, mix_gain, pool_weight, pool_scale):
    floats = local_part.astype(jnp.float32)
    squares = lax.psum(jnp.sum(floats * floats, axis=-1).astype(jnp.bfloat16), "tp").astype(
        jnp.float32
    )
    normed = (
        floats * lax.rsqrt(squares[..., None] / D + epsilon) * mix_gain.astype(jnp.float32)
    ).astype(jnp.bfloat16)
    seq_count, seq_length, part_width = local_part.shape
    groups_here = pool_weight.shape[0]
    group_width = pool_weight.shape[1]
    grouped = normed.astype(jnp.float32).reshape(seq_count, seq_length, groups_here, group_width)
    group_ids = lax.axis_index("tp") * groups_here + jnp.arange(groups_here, dtype=jnp.int32)
    windows = 2 ** (group_ids + 1)
    pooled = trailing(grouped, windows, 2**GROUPS)
    diff = (pooled - grouped).astype(jnp.bfloat16)

    def mix_cols(block_cols, offset):
        return jnp.einsum("bsgc,gcd->bsgd", diff, block_cols, preferred_element_type=jnp.float32)

    mixed = over_all(pool_weight, "fs", 2, mix_cols)
    mixed = mixed.reshape(seq_count, seq_length, part_width)
    return (floats + mixed * pool_scale.astype(jnp.float32)).astype(jnp.bfloat16)


def local(
    tokens,
    pre_gain,
    first_gate,
    first_up,
    first_down,
    mix_gain,
    pool_weight,
    pool_scale,
    post_gain,
    second_gate,
    second_up,
    second_down,
):
    first_out = half_step(tokens, pre_gain, first_gate, first_up, first_down)
    after_first = (tokens.astype(jnp.float32) + 0.5 * first_out).astype(jnp.bfloat16)
    after_mix = pool_mix(after_first, mix_gain, pool_weight, pool_scale)
    second_out = half_step(after_mix, post_gain, second_gate, second_up, second_down)
    return (after_mix.astype(jnp.float32) + 0.5 * second_out).astype(jnp.bfloat16)


def solution(mesh):
    placed = (
        P(("rep", "fs"), None, "tp"),
        P(),
        P("fs", "tp"),
        P("fs", "tp"),
        P("tp", "fs"),
        P("tp"),
        P("tp", None, "fs"),
        P("tp"),
        P(),
        P("fs", "tp"),
        P("fs", "tp"),
        P("tp", "fs"),
    )
    return jax.shard_map(
        local, mesh=mesh, in_specs=placed, out_specs=P(("rep", "fs"), None, "tp"), check_vma=False
    )
```

profile of v0, /device:TPU:1, one launch (start us, length us, event | category | flops | bytes accessed | tf_op | source)
XLA Modules:
  0.0 984.1 jit_solution(10474154368155014482)
XLA Ops:
  6.5 0.7 all-gather.7.cloned.1.call-update
  7.3 0.7 all-gather.11.cloned.1.call-update
  8.1 0.7 all-gather.9.cloned.1.call-update
  8.8 3.4 all_gather.27
  12.4 131.5 %all-gather.7.cloned.1.call-done = bf16[1024,1280]{1,0:T(8,128)(2,1)} async-done(((bf16[32,1280]{1,0:T(8,128)(2,1)}), bf16[1024,1280]{1,0:T(8,128)(2,1)}) %all-gather.7.cloned.1.call-update) | async-done | bytes 2621456 | tf_op jit(solution)/shard_map/all_gather | solution.py:14
  143.9 2.6 fusion.55
  146.6 152.8 %all-gather.11.cloned.1.call-done = bf16[1280,1024]{0,1:T(8,128)(2,1)} async-done(((bf16[1280,32]{0,1:T(8,128)(2,1)}), bf16[1280,1024]{0,1:T(8,128)(2,1)}) %all-gather.11.cloned.1.call-update) | async-done | bytes 2621456 | tf_op jit(solution)/shard_map/all_gather | solution.py:19
  299.3 155.2 %all-gather.9.cloned.1.call-done = bf16[1024,1280]{1,0:T(8,128)(2,1)} async-done(((bf16[32,1280]{1,0:T(8,128)(2,1)}), bf16[1024,1280]{1,0:T(8,128)(2,1)}) %all-gather.9.cloned.1.call-update) | async-done | bytes 2621456 | tf_op jit(solution)/shard_map/all_gather | solution.py:14
  454.5 5.0 convolution_convert_fusion.1
  459.6 0.5 all-gather.13.cloned.1.call-update
  460.7 0.7 all-gather.17.cloned.1.call-update
  461.7 68.0 %all_gather.31 = bf16[2,256,256]{1,2,0:T(8,128)(2,1)S(1)} all-gather(bf16[2,256,8]{1,2,0:T(8,128)(2,1)S(1)} %copy-done.4), channel_id=1, replica_groups=mesh['rep'=2,'fs'=32,'tp'=2] {'fs'}, dimensions={2}, use_global_device_ids=true | all-gather | bytes 270336 | tf_op jit(solution)/shard_map/all_gather | solution.py:19
  529.8 1.1 fusion.40
  530.9 38.9 %psum.7 = bf16[1,256]{1,0:T(2,128)(2,1)S(1)} all-reduce(bf16[1,256]{1,0:T(2,128)(2,1)S(1)} %convert_element_type.125), channel_id=1, replica_groups=mesh['rep'=2,'fs'=32,'tp'=2] {'tp'}, use_global_device_ids=true, to_apply=%region_3.4 | all-reduce | flops 256 | bytes 1024 | tf_op jit(solution)/shard_map/psum | solution.py:66
  569.8 1.1 fusion.46
  571.0 1.8 fusion.47
  573.1 2.2 all_gather.32
  575.5 51.3 %all-gather.13.cloned.1.call-done = bf16[1024,1280]{1,0:T(8,128)(2,1)} async-done(((bf16[32,1280]{1,0:T(8,128)(2,1)}), bf16[1024,1280]{1,0:T(8,128)(2,1)}) %all-gather.13.cloned.1.call-update) | async-done | bytes 2621456 | tf_op jit(solution)/shard_map/all_gather | solution.py:14
  626.9 2.6 fusion.51
  629.5 152.5 %all-gather.15.cloned.1.call-done = bf16[1024,1280]{1,0:T(8,128)(2,1)} async-done(((bf16[32,1280]{1,0:T(8,128)(2,1)}), bf16[1024,1280]{1,0:T(8,128)(2,1)}) %all-gather.15.cloned.1.call-update) | async-done | bytes 2621456 | tf_op jit(solution)/shard_map/all_gather | solution.py:14
  782.0 155.5 %all-gather.17.cloned.1.call-done = bf16[1280,1024]{0,1:T(8,128)(2,1)} async-done(((bf16[1280,32]{0,1:T(8,128)(2,1)}), bf16[1280,1024]{0,1:T(8,128)(2,1)}) %all-gather.17.cloned.1.call-update) | async-done | bytes 2621456 | tf_op jit(solution)/shard_map/all_gather | solution.py:19
  937.5 4.9 convolution_convert_fusion
  942.5 33.1 %reduce-scatter.5.cloned.1.call-done = bf16[256,512]{1,0:T(8,128)(2,1)} async-done(((bf16[256,1024]{1,0:T(8,128)(2,1)}), bf16[256,512]{1,0:T(8,128)(2,1)}) %reduce-scatter.5.cloned.1.call-update) | async-done | bytes 262160 | tf_op jit(solution)/shard_map/reduce_scatter | solution.py:47
  975.5 1.7 fusion.44
  (46 shorter events, 1.9 us)
Async XLA Ops:
  6.5 137.3 %all-gather.7.cloned.1.call-start = ((), (), s32[]{:S(2)}) async-start(), calls=%async_computation.2 | async-start | bytes 2703360 | tf_op jit(solution)/shard_map/all_gather | solution.py:14
  7.3 292.1 %all-gather.11.cloned.1.call-start = ((), (), s32[]{:S(2)}) async-start(), calls=%async_computation.4 | async-start | bytes 2703360 | tf_op jit(solution)/shard_map/all_gather | solution.py:19
  8.0 446.5 %all-gather.9.cloned.1.call-start = ((), (), s32[]{:S(2)}) async-start(), calls=%async_computation.3 | async-start | bytes 2703360 | tf_op jit(solution)/shard_map/all_gather | solution.py:14
  8.7 521.0 %reduce-scatter.3.cloned.1.call-start = ((), (), s32[]{:S(2)}) async-start(), calls=%async_computation.5 | async-start | bytes 786432 | tf_op jit(solution)/shard_map/reduce_scatter | solution.py:47
  12.2 442.3 %copy-start.2 = (f32[1024]{0:T(1024)S(1)}, f32[1024]{0:T(1024)}, u32[]{:S(2)}) copy-start(f32[1024]{0:T(1024)} %param.13) | copy-start | bytes 12292
  146.5 315.2 %copy-start.4 = (bf16[2,256,8]{1,2,0:T(8,128)(2,1)S(1)}, bf16[2,256,8]{1,2,0:T(8,128)(2,1)}, u32[]{:S(2)}) copy-start(bf16[2,256,8]{1,2,0:T(8,128)(2,1)} %param.18) | copy-start | bytes 24580
  146.5 383.3 %copy-start = (bf16[1,256,512]{2,1,0:T(8,128)(2,1)S(1)}, bf16[1,256,512]{2,1,0:T(8,128)(2,1)}, u32[]{:S(2)}) copy-start(bf16[1,256,512]{2,1,0:T(8,128)(2,1)} %param.12) | copy-start | bytes 786436
  146.5 423.3 %copy-start.5 = (f32[512]{0:T(512)S(1)}, f32[512]{0:T(512)}, u32[]{:S(2)}) copy-start(f32[512]{0:T(512)} %param.17) | copy-start | bytes 6148
  459.5 167.3 %all-gather.13.cloned.1.call-start = ((), (), s32[]{:S(2)}) async-start(), calls=%async_computation.6 | async-start | bytes 2703360 | tf_op jit(solution)/shard_map/all_gather | solution.py:14
  460.1 321.9 %all-gather.15.cloned.1.call-start = ((), (), s32[]{:S(2)}) async-start(), calls=%async_computation.7 | async-start | bytes 2703360 | tf_op jit(solution)/shard_map/all_gather | solution.py:14
  460.7 476.8 %all-gather.17.cloned.1.call-start = ((), (), s32[]{:S(2)}) async-start(), calls=%async_computation.8 | async-start | bytes 2703360 | tf_op jit(solution)/shard_map/all_gather | solution.py:19
  461.4 514.1 %reduce-scatter.5.cloned.1.call-start = ((), (), s32[]{:S(2)}) async-start(), calls=%async_computation.9 | async-start | bytes 786432 | tf_op jit(solution)/shard_map/reduce_scatter | solution.py:47
  571.0 2.0 copy-start.1
  571.0 2.0 copy-start.6
  572.8 54.1 %copy-start.3 = (f32[1024]{0:T(1024)S(1)}, f32[1024]{0:T(1024)}, u32[]{:S(2)}) copy-start(f32[1024]{0:T(1024)} %param.20) | copy-start | bytes 12292
Sparse Core Ops, SparseCore 0:
  9.0 134.8 all-gather.6
  145.5 153.7 all-gather.10
  301.0 153.4 all-gather.8
  459.6 33.0 reduce-scatter.2
  494.2 132.6 all-gather.12
  628.4 153.6 all-gather.14
  783.7 153.7 all-gather.16
  942.6 32.8 reduce-scatter.4
where the time goes:
time: 984 us
  waiting for transfers between devices  836 us (85%)
  blocking collectives  112 us (11%)
  matrix products  17 us (2%)
  between operations  13.7 us (1%)
    all_gather x4, waiting for transfers between devices, taken_in(): lax.all_gather(part, axis, axis=dim, tiled=True)  491 us
    all_gather x2, waiting for transfers between devices, over_all(): whole = lax.all_gather(shard, axis, axis=dim, tiled=True)  308 us
    all_gather x1, blocking collectives, over_all(): whole = lax.all_gather(shard, axis, axis=dim, tiled=True)  68 us
    psum x1, blocking collectives, pool_mix(): lax.psum(jnp.sum(floats * floats, axis=-1).astype(jnp.bfloat16), 'tp')  38.9 us
    reduce_scatter x2, waiting for transfers between devices, half_step(): lax.psum_scatter(partial_value.astype(jnp.bfloat16), 'tp', scatter_dimens...  33.1 us
  transfers between devices with their start and end apart: 8, of which 7 were waited for; matrix products, arithmetic and copies ran while one was open for 1% of the time, Pallas kernels for 0%

commit v1 on v0

v1 whole, which is shorter than its diff:
```python
import jax
import jax.numpy as jnp
from jax import lax
from jax.experimental import pallas as pl
from jax.experimental.pallas import tpu as pltpu
from jax.sharding import PartitionSpec as P

MESH = pl.DeviceIdType.MESH
BF16 = jnp.bfloat16
F32 = jnp.float32
EPS = 1e-06
D = 1024
HALF = 512
ROWS = 128
UNIT = 640
N_SEND = 224
N_RECV = 224
N_LOCAL = 16


class Net:
    def __init__(self, ss, rs, ls, here):
        self.ss, self.rs, self.ls, self.here = ss, rs, ls, here
        self.names = {}
        self.sends = 0
        self.locals = 0
        self.pending = []

    def name(self, key, width=1):
        if key not in self.names:
            self.names[key] = sum(w for _, w in self.names.values()), width
        return self.names[key][0]

    def send(self, key, make, cond=None, width=1, shift=None):
        base = self.name(key, width)
        slot = self.sends
        self.sends += 1

        def copy():
            src, dst, device = make()
            where = base if shift is None else base + shift
            return pltpu.make_async_remote_copy(
                src, dst, self.ss.at[slot], self.rs.at[where], device_id=device, device_id_type=MESH
            )

        def end():
            copy().wait_send()

        if cond is None:
            copy().start()
            self.pending.append(end)
        else:
            pl.when(cond)(lambda: copy().start())
            self.pending.append(lambda: pl.when(cond)(end))

    def recv(self, key, ref, offset=0, width=1):
        where = self.name(key, width) + offset
        pltpu.make_async_remote_copy(
            ref, ref, self.ss.at[0], self.rs.at[where], device_id=self.here, device_id_type=MESH
        ).wait_recv()

    def local(self, src, dst):
        copy = pltpu.make_async_copy(src, dst, self.ls.at[self.locals])
        self.locals += 1
        return copy

    def finish(self):
        assert self.sends <= N_SEND and self.locals <= N_LOCAL
        assert sum(w for _, w in self.names.values()) <= N_RECV
        for end in self.pending:
            end()


class Stream:
    def __init__(self, net, tag, piece, group, first, second, sibling):
        self.net, self.tag, self.piece, self.group = net, tag, piece, group
        self.a, self.ap, self.am, self.ao, self.to_ap, self.to_am = first
        self.b, self.bp, self.bm, self.bo, self.to_bp, self.to_bm = second
        self.sibling = sibling

    def send(self, what, a, b, device):
        self.net.send((self.tag, what), lambda: (self.piece(a, b), self.piece(a, b), device))

    def recv(self, what, a, b):
        self.net.recv((self.tag, what), self.piece(a, b))

    def both(self, k, a):
        self.send(f"2m{k}", a, self.b, self.to_bp)
        self.send(f"2p{k}", a, self.b, self.to_bm)

    def hand(self, what, b):
        self.net.send((self.tag, what), lambda: (self.group(b), self.group(b), self.sibling))

    def one(self):
        self.send("1m", self.a, self.b, self.to_ap)
        self.send("1p", self.a, self.b, self.to_am)
        self.both(0, self.a)

    def two(self):
        self.recv("1m", self.am, self.b)
        self.send("1o", self.am, self.b, self.to_ap)
        self.both(1, self.am)
        self.recv("1p", self.ap, self.b)
        self.both(2, self.ap)

    def three(self):
        self.recv("1o", self.ao, self.b)
        self.both(3, self.ao)
        self.hand("d0", self.b)

    def four(self):
        self.recv("2m0", self.a, self.bm)
        self.send("2o0", self.a, self.bm, self.to_bp)
        self.recv("2m1", self.am, self.bm)
        self.send("2o1", self.am, self.bm, self.to_bp)
        self.recv("2p2", self.ap, self.bp)
        self.send("2o2", self.ap, self.bp, self.to_bm)
        self.recv("2p3", self.ao, self.bp)
        self.send("2o3", self.ao, self.bp, self.to_bm)
        self.recv("2p0", self.a, self.bp)
        self.recv("2p1", self.am, self.bp)
        self.hand("dp", self.bp)
        self.recv("2m2", self.ap, self.bm)
        self.recv("2m3", self.ao, self.bm)
        self.hand("dm", self.bm)

    def five(self):
        self.recv("2o0", self.a, self.bo)
        self.recv("2o1", self.am, self.bo)
        self.recv("2o2", self.ap, self.bo)
        self.recv("2o3", self.ao, self.bo)
        self.hand("do", self.bo)

    def handed(self, other):
        for what, b in (("d0", self.b), ("dp", self.bp), ("dm", self.bm), ("do", self.bo)):
            self.net.recv((self.tag, what), other(b))


def normed(values, gain):
    floats = values.astype(F32)
    mean = jnp.mean(floats * floats, axis=-1, keepdims=True)
    return (floats * lax.rsqrt(mean + EPS) * gain).astype(BF16)


def kernel(
    tok, g1, gate1, up1, down1, mixg, pool, scale, g2, gate2, up2, down2, out,
    w, pw, xt, xq, n, h, acc, pm, pp, so, sm, sp, ra, rb, a1, hs, hr, mg, ob, sq, rq, oc, of, ss, rs, ls,
):
    rep = lax.axis_index("rep")
    fs = lax.axis_index("fs")
    c = lax.axis_index("tp")
    o = 1 - c
    j = lax.div(fs, 16)
    z = rep * 2 + j
    y = lax.rem(lax.div(fs, 4), 4)
    x = lax.rem(fs, 4)
    zp, zo, zm = (lax.rem(z + k, 4) for k in (1, 2, 3))
    yp, yo, ym = (lax.rem(y + k, 4) for k in (1, 2, 3))
    xp, xo, xm = (lax.rem(x + k, 4) for k in (1, 2, 3))

    def dev(z_, y_, x_, c_):
        return (lax.div(z_, 2), lax.rem(z_, 2) * 16 + y_ * 4 + x_, c_)

    sibling = dev(z, y, x, o)
    net = Net(ss, rs, ls, sibling)
    keeper = c == j
    taker = c != j
    zq = lax.rem(z + 1 + 2 * lax.rem(z + c, 2), 4)
    peer = dev(zq, y, x, c)

    def cols(k):
        return pl.ds(pl.multiple_of(k * UNIT, 128), UNIT)

    def feats(k):
        return pl.ds(pl.multiple_of(k * HALF, 128), HALF)

    def rows(k):
        return pl.ds(pl.multiple_of(k * ROWS, 128), ROWS)

    mats = ((gate1, up1, down1), (gate2, up2, down2), (gate2, up2, down2))
    subs = (lax.div(z, 2), 0, 1)

    own_tok = net.local(tok.at[rows(c), :], xt.at[z, :, feats(c)])
    own_tok.start()
    own_w = []
    for u in range(3):
        base = net.locals
        net.locals += 3
        own_w.append(base)

    def own_copy(u, m):
        return pltpu.make_async_copy(
            mats[u][m].at[:, cols(subs[u])], w.at[u, m, c, y, x], ls.at[own_w[u] + m]
        )

    base_pool = net.locals
    net.locals += 1

    def own_pool():
        return pltpu.make_async_copy(pool, pw.at[c, c, y, x], ls.at[base_pool])

    @pl.when(keeper)
    def _():
        for u in range(3):
            for m in range(3):
                own_copy(u, m).start()
        own_pool().start()

    own_mg = net.local(mixg, mg.at[0, c])
    own_sc = net.local(scale, mg.at[1, c])
    own_mg.start()
    own_sc.start()

    barrier = pltpu.get_barrier_semaphore()
    friends = [dev(z, y, xp, c), dev(z, y, xm, c), dev(z, yp, x, c), dev(z, ym, x, c), sibling]
    friends += [dev(z_, y, x, k) for z_ in (zp, zm) for k in range(2)]
    for friend in friends:
        pl.semaphore_signal(barrier, inc=1, device_id=friend, device_id_type=MESH)
    pl.semaphore_wait(barrier, len(friends))

    def exchange(u):
        for ab, z_ in ((0, zp), (1, zm)):
            sub = (lax.div(z_, 2), 0, 1)[u]
            part = pl.ds(16 * ab, 16)
            for m in range(3):
                net.send(
                    ("z", u, ab, m),
                    lambda m=m, part=part, sub=sub, z_=z_: (
                        mats[u][m].at[part, cols(sub)],
                        w.at[u, m, o, y, x, part, :],
                        dev(z_, y, x, o),
                    ),
                    cond=taker,
                )

    def own(u):
        @pl.when(keeper)
        def _():
            for m in range(3):
                own_copy(u, m).wait()

        @pl.when(taker)
        def _():
            for ab in range(2):
                for m in range(3):
                    net.recv(("z", u, ab, m), w.at[u, m, c, y, x, pl.ds(16 * ab, 16), :])

    in_x = (x, xp, xm, xo, dev(z, y, xp, c), dev(z, y, xm, c))
    in_y = (y, yp, ym, yo, dev(z, yp, x, c), dev(z, ym, x, c))

    def stream_a(u):
        return Stream(
            net, ("a", u),
            lambda a, b: w.at[u, :, c, b, a, pl.ds(0, 16), :],
            lambda b: w.at[u, :, c, b, :, pl.ds(0, 16), :],
            in_x, in_y, sibling,
        )

    def stream_b(u):
        return Stream(
            net, ("b", u),
            lambda a, b: w.at[u, :, c, a, b, pl.ds(16, 16), :],
            lambda b: w.at[u, :, c, :, b, pl.ds(16, 16), :],
            in_y, in_x, sibling,
        )

    sa = [stream_a(u) for u in range(3)]
    sb = [stream_b(u) for u in range(3)]
    spool = Stream(
        net, ("p",),
        lambda a, b: pw.at[:, c, b, a],
        lambda b: pw.at[:, c, b],
        in_x, in_y, sibling,
    )

    def handed(u):
        sa[u].handed(lambda b: w.at[u, :, o, b, :, pl.ds(0, 16), :])
        sb[u].handed(lambda b: w.at[u, :, o, :, b, pl.ds(16, 16), :])

    def spread_tokens():
        net.send("ts", lambda: (tok.at[rows(o), :], xt.at[z, :, feats(c)], sibling))
        for k in range(2):
            for key, z_ in (("tm", zp), ("tp", zm)):
                net.send(
                    key,
                    lambda k=k, z_=z_: (tok.at[rows(k), :], xt.at[z, :, feats(c)], dev(z_, y, x, k)),
                    width=2, shift=c,
                )

    def relay_tokens():
        net.recv("tm", xt.at[zm, :, feats(0)], 0, 2)
        net.send("to0", lambda: (xt.at[zm, :, feats(0)], xt.at[zm, :, feats(0)], dev(zp, y, x, c)))
        net.recv("tp", xt.at[zp, :, feats(1)], 1, 2)
        net.send("to1", lambda: (xt.at[zp, :, feats(1)], xt.at[zp, :, feats(1)], dev(zm, y, x, c)))
        net.recv("tm", xt.at[zm, :, feats(1)], 1, 2)
        net.recv("tp", xt.at[zp, :, feats(0)], 0, 2)

    def gate_up(u, count):
        def step(k, carry):
            part = pl.ds(pl.multiple_of(k * 128, 128), 128)
            wg = w[u, 0, :, :, :, :, part].reshape(D, 128)
            wu = w[u, 1, :, :, :, :, part].reshape(D, 128)
            both = jnp.dot(
                n[pl.ds(0, count), :], jnp.concatenate([wg, wu], axis=1), preferred_element_type=F32
            )
            gate, up = both[:, :128], both[:, 128:]
            h[pl.ds(0, count), part] = (gate * jax.nn.sigmoid(gate) * up).astype(BF16)
            return carry

        lax.fori_loop(0, UNIT // 128, step, 0)

    def down(u, start, count, put):
        def step(k, carry):
            wd = w[u, 2, lax.div(k, 2), pl.ds(lax.rem(k, 2) * 2, 2), :, :, :].reshape(256, UNIT)
            part = lax.dot_general(
                h[pl.ds(start, count), :], wd, (((1,), (1,)), ((), ())), preferred_element_type=F32
            )
            put(pl.ds(pl.multiple_of(k * 256, 256), 256), part)
            return carry

        lax.fori_loop(0, 4, step, 0)

    exchange(0)
    spread_tokens()
    own(0)
    sa[0].one()
    sb[0].one()
    exchange(1)
    exchange(2)
    net.send("ps", lambda: (pool, pw.at[c, o, y, x], sibling), cond=taker)
    net.send("pz", lambda: (pool, pw.at[c, j, y, x], dev(zp, y, x, j)), width=2, shift=c)
    own_mg.wait()
    own_sc.wait()
    net.send("mg", lambda: (mixg, mg.at[0, c], sibling))
    net.send("sc", lambda: (scale, mg.at[1, c], sibling))

    sa[0].two()
    sb[0].two()
    gain1 = g1[...]
    own_tok.wait()
    net.recv("ts", xt.at[z, :, feats(o)])
    n[pl.ds(0, ROWS), :] = normed(xt[z], gain1)
    sa[0].three()
    sb[0].three()
    relay_tokens()
    own(1)
    sa[1].one()
    sb[1].one()
    n[pl.ds(ROWS, ROWS), :] = normed(xt[zm], gain1)
    n[pl.ds(2 * ROWS, ROWS), :] = normed(xt[zp], gain1)
    sa[0].four()
    sb[0].four()
    sa[1].two()
    sb[1].two()

    @pl.when(keeper)
    def _():
        own_pool().wait()
        net.recv("ps", pw.at[o, c, y, x])

    @pl.when(taker)
    def _():
        net.recv("pz", pw.at[0, c, y, x], 0, 2)
        net.recv("pz", pw.at[1, c, y, x], 1, 2)

    spool.one()
    sa[1].three()
    sb[1].three()
    net.recv("to0", xt.at[zo, :, feats(0)])
    net.recv("to1", xt.at[zo, :, feats(1)])
    n[pl.ds(3 * ROWS, ROWS), :] = normed(xt[zo], gain1)
    sa[0].five()
    sb[0].five()
    own(2)
    sa[2].one()
    sb[2].one()
    spool.two()
    handed(0)

    gate_up(0, 4 * ROWS)
    spool.three()
    sa[1].four()
    sb[1].four()

    def put_opposite(part, value):
        so[:, part] = value.astype(BF16)

    down(0, 3 * ROWS, ROWS, put_opposite)
    net.send("r0", lambda: (so.at[:, feats(0)], ra.at[0], dev(zp, y, x, c)))
    net.send("r1", lambda: (so.at[:, feats(1)], ra.at[1], dev(zm, y, x, c)))

    def put_rest(part, value):
        acc[pl.ds(0, ROWS), part] = value[:ROWS]
        pm[:, part] = value[ROWS : 2 * ROWS]
        pp[:, part] = value[2 * ROWS :]

    down(0, 0, 3 * ROWS, put_rest)
    sp[:, HALF:] = pp[:, HALF:].astype(BF16)
    sm[:, :HALF] = pm[:, :HALF].astype(BF16)
    sa[2].two()
    sb[2].two()
    net.send("qm1", lambda: (sp.at[:, feats(1)], rb.at[0, :, feats(1)], dev(zp, y, x, c)))
    net.send("qp0", lambda: (sm.at[:, feats(0)], rb.at[1, :, feats(0)], dev(zm, y, x, c)))
    net.recv("r0", ra.at[0])
    sp[:, :HALF] = (pp[:, :HALF] + ra[0].astype(F32)).astype(BF16)
    net.recv("r1", ra.at[1])
    sm[:, HALF:] = (pm[:, HALF:] + ra[1].astype(F32)).astype(BF16)
    sa[2].three()
    net.send("qm0", lambda: (sp.at[:, feats(0)], rb.at[0, :, feats(0)], dev(zp, y, x, c)))
    net.send("qp1", lambda: (sm.at[:, feats(1)], rb.at[1, :, feats(1)], dev(zm, y, x, c)))
    sb[2].three()
    spool.four()
    sa[1].five()
    sb[1].five()
    spool.five()
    sa[2].four()
    sb[2].four()
    for key, k, half in (("qm", 0, 1), ("qp", 1, 0), ("qm", 0, 0), ("qp", 1, 1)):
        net.recv(f"{key}{half}", rb.at[k, :, feats(half)])
    block = acc[pl.ds(0, ROWS), :] + rb[0].astype(F32) + rb[1].astype(F32)
    a1[...] = (xt[z].astype(F32) + 0.5 * block).astype(BF16)

    net.recv("mg", mg.at[0, o])
    net.recv("sc", mg.at[1, o])
    mix_gain = jnp.concatenate([mg[0, 0], mg[0, 1]], axis=1)
    mix_scale = jnp.concatenate([mg[1, 0], mg[1, 1]], axis=1)
    hidden = normed(a1[...], mix_gain)
    hs[...] = hidden
    spool.handed(lambda b: pw.at[:, o, b])
    net.send("h", lambda: (hs.at[pl.ds(112, 16), :], hr, sibling))
    sa[2].five()
    sb[2].five()
    net.recv("h", hr)
    before = jnp.where(c == 1, hr[...].astype(F32), 0.0)
    floats = hs[...].astype(F32)
    longer = jnp.concatenate([before, floats], axis=0)
    positions = c * ROWS + lax.broadcasted_iota(jnp.int32, (ROWS, 256), 0)
    for g in range(4):
        lanes = slice(256 * g, 256 * g + 256)
        total = longer[:, lanes]
        for k in range(g + 1):
            total = total + pltpu.roll(total, 2**k, axis=0)
        counts = jnp.minimum(positions + 1, 2 ** (g + 1)).astype(F32)
        diff = (total[16:] / counts - floats[:, lanes]).astype(BF16)
        wide = pw[g // 2].reshape(32, 16, 256).astype(F32)
        maps = wide[:, 8 * (g % 2) : 8 * (g % 2) + 8, :].reshape(256, 256).astype(BF16)
        mixed = lax.dot_general(diff, maps, (((1,), (1,)), ((), ())), preferred_element_type=F32)
        after = a1[:, lanes].astype(F32) + mixed * mix_scale[:, lanes]
        ob[:, lanes] = after.astype(BF16)

    net.send("a", lambda: (ob, xq, peer))
    gain2 = g2[...]
    n[pl.ds(0, ROWS), :] = normed(ob[...], gain2)
    handed(1)
    net.recv("a", xq)
    n[pl.ds(ROWS, ROWS), :] = normed(xq[...], gain2)

    def put_first(part, value):
        acc[:, part] = value

    def put_second(part, value):
        acc[:, part] += value

    gate_up(1, 2 * ROWS)
    down(1, 0, 2 * ROWS, put_first)
    handed(2)
    gate_up(2, 2 * ROWS)
    down(2, 0, 2 * ROWS, put_second)
    sq[...] = acc[pl.ds(ROWS, ROWS), :].astype(BF16)
    net.send("b", lambda: (sq, rq, peer))
    net.recv("b", rq)
    block = acc[pl.ds(0, ROWS), :] + rq[...].astype(F32)
    oc[...] = (ob[...].astype(F32) + 0.5 * block).astype(BF16)
    net.send("f", lambda: (oc.at[:, feats(o)], of, sibling))
    out[rows(c), :] = oc[:, feats(c)]
    net.recv("f", of)
    out[rows(o), :] = of[...]
    net.finish()


def local(tok, g1, gate1, up1, down1, mixg, pool, scale, g2, gate2, up2, down2):
    hbm = pl.BlockSpec(memory_space=pl.ANY)
    vmem = pl.BlockSpec(memory_space=pltpu.VMEM)
    result = pl.pallas_call(
        kernel,
        out_shape=jax.ShapeDtypeStruct((256, HALF), BF16),
        in_specs=[hbm, vmem, hbm, hbm, hbm, hbm, hbm, hbm, vmem, hbm, hbm, hbm],
        out_specs=vmem,
        scratch_shapes=[
            pltpu.VMEM((3, 3, 2, 4, 4, 32, UNIT), BF16),
            pltpu.VMEM((2, 2, 4, 4, 16, 256), BF16),
            pltpu.VMEM((4, ROWS, D), BF16),
            pltpu.VMEM((ROWS, D), BF16),
            pltpu.VMEM((4 * ROWS, D), BF16),
            pltpu.VMEM((4 * ROWS, UNIT), BF16),
            pltpu.VMEM((2 * ROWS, D), F32),
            pltpu.VMEM((ROWS, D), F32),
            pltpu.VMEM((ROWS, D), F32),
            pltpu.VMEM((ROWS, D), BF16),
            pltpu.VMEM((ROWS, D), BF16),
            pltpu.VMEM((ROWS, D), BF16),
            pltpu.VMEM((2, ROWS, HALF), BF16),
            pltpu.VMEM((2, ROWS, D), BF16),
            pltpu.VMEM((ROWS, D), BF16),
            pltpu.VMEM((ROWS, D), BF16),
            pltpu.VMEM((16, D), BF16),
            pltpu.VMEM((2, 2, 1, HALF), F32),
            pltpu.VMEM((ROWS, D), BF16),
            pltpu.VMEM((ROWS, D), BF16),
            pltpu.VMEM((ROWS, D), BF16),
            pltpu.VMEM((ROWS, D), BF16),
            pltpu.VMEM((ROWS, HALF), BF16),
            pltpu.SemaphoreType.DMA((N_SEND,)),
            pltpu.SemaphoreType.DMA((N_RECV,)),
            pltpu.SemaphoreType.DMA((N_LOCAL,)),
        ],
        compiler_params=pltpu.CompilerParams(collective_id=0, has_side_effects=True, vmem_limit_bytes=48 * 2**20),
    )(
        tok.reshape(256, HALF), g1.reshape(1, D), gate1, up1, down1.T, mixg.reshape(1, HALF),
        pool.transpose(0, 2, 1).reshape(16, 256), scale.reshape(1, HALF), g2.reshape(1, D), gate2, up2, down2.T,
    )
    return result.reshape(1, 256, HALF)


def solution(mesh):
    placed = (
        P(("rep", "fs"), None, "tp"),
        P(),
        P("fs", "tp"),
        P("fs", "tp"),
        P("tp", "fs"),
        P("tp"),
        P("tp", None, "fs"),
        P("tp"),
        P(),
        P("fs", "tp"),
        P("fs", "tp"),
        P("tp", "fs"),
    )
    return jax.shard_map(
        local, mesh=mesh, in_specs=placed, out_specs=P(("rep", "fs"), None, "tp"), check_vma=False
    )
```

time: 984 us -> 85 us (0.09)
  waiting for transfers between devices: 836 us -> 0 us
  blocking collectives: 112 us -> 0 us
  Pallas kernels: 0 us -> 75.5 us
  matrix products: 17 us -> 0 us
  between operations: 13.7 us -> 0.02 us
    all_gather x6 -> x0, waiting for transfers between devices: 799 us -> none  [the longest x4 491 us: taken_in(): lax.all_gather(part, axis, axis=dim, tiled=True)]
    pallas_call x0 -> x1, Pallas kernels: none -> 75.5 us  [local(): pl.pallas_call(kernel, out_shape=jax.ShapeDtypeStruct((256, HALF), BF16),...]
    all_gather x3 -> x0, blocking collectives: 73.6 us -> none  [the longest x1 68 us: over_all(): whole = lax.all_gather(shard, axis, axis=dim, tiled=True)]
    psum x1 -> x0, blocking collectives: 38.9 us -> none  [pool_mix(): lax.psum(jnp.sum(floats * floats, axis=-1).astype(jnp.bfloat16), 'tp')]
    reduce_scatter x2 -> x0, waiting for transfers between devices: 33.1 us -> none  [half_step(): lax.psum_scatter(partial_value.astype(jnp.bfloat16), 'tp', scatter_dimens...]
    dot_general x5 -> x0, matrix products: 17 us -> none  [the longest x2 9.93 us: project(): return jnp.dot(hidden, block_cols, preferred_element_type=jnp.float32)]
  transfers between devices with their start and end apart: 8 -> 0, of which waited for: 7 -> 0; matrix products, arithmetic and copies ran while one was open for 1% -> 0% of each run, Pallas kernels for 0% -> 0%
where the time goes in v1:
time: 85 us; the launch traced here: 84.6 us
  Pallas kernels  75.5 us (89%)
  local copies, waits for them, and re-layouts  9.05 us (11%)
    pallas_call x1, Pallas kernels, local(): pl.pallas_call(kernel, out_shape=jax.ShapeDtypeStruct((256, HALF), BF16),...  75.5 us
    unnamed x25, local copies, waits for them, and re-layouts  9.05 us

profile of v1, /device:TPU:1, one launch (start us, length us, event | category | flops | bytes accessed | tf_op | source)
XLA Modules:
  0.0 84.6 jit_solution(10188631155031459416)
XLA Ops:
  0.0 0.0 copy-start.7
  0.0 0.0 copy-start.8
  0.0 0.0 copy-start.10
  0.0 0.7 copy-done.7
  0.7 0.0 copy-done.8
  0.7 0.0 copy-done.10
  0.7 0.0 copy-start
  0.7 0.9 %copy-done = bf16[1,256,512]{2,1,0:T(8,128)(2,1)S(1)} copy-done((bf16[1,256,512]{2,1,0:T(8,128)(2,1)S(1)}, bf16[1,256,512]{2,1,0:T(8,128)(2,1)}, u32[]{:S(2)}) %copy-start) | copy-done | bytes 262168
  1.7 0.0 copy-start.1
  1.7 0.9 %copy-done.1 = bf16[32,1280]{1,0:T(8,128)(2,1)S(1)} copy-done((bf16[32,1280]{1,0:T(8,128)(2,1)S(1)}, bf16[32,1280]{1,0:T(8,128)(2,1)}, u32[]{:S(2)}) %copy-start.1) | copy-done | bytes 81944
  2.6 0.0 copy-start.2
  2.6 0.9 %copy-done.2 = bf16[32,1280]{1,0:T(8,128)(2,1)S(1)} copy-done((bf16[32,1280]{1,0:T(8,128)(2,1)S(1)}, bf16[32,1280]{1,0:T(8,128)(2,1)}, u32[]{:S(2)}) %copy-start.2) | copy-done | bytes 81944
  3.4 0.0 copy-start.3
  3.4 0.9 %copy-done.3 = bf16[1280,32]{0,1:T(8,128)(2,1)S(1)} copy-done((bf16[1280,32]{0,1:T(8,128)(2,1)S(1)}, bf16[1280,32]{0,1:T(8,128)(2,1)}, u32[]{:S(2)}) %copy-start.3) | copy-done | bytes 81944
  4.3 0.0 copy-start.4
  4.3 0.9 %copy-done.4 = bf16[32,1280]{1,0:T(8,128)(2,1)S(1)} copy-done((bf16[32,1280]{1,0:T(8,128)(2,1)S(1)}, bf16[32,1280]{1,0:T(8,128)(2,1)}, u32[]{:S(2)}) %copy-start.4) | copy-done | bytes 81944
  5.2 0.0 copy-start.5
  5.2 0.9 %copy-done.5 = bf16[32,1280]{1,0:T(8,128)(2,1)S(1)} copy-done((bf16[32,1280]{1,0:T(8,128)(2,1)S(1)}, bf16[32,1280]{1,0:T(8,128)(2,1)}, u32[]{:S(2)}) %copy-start.5) | copy-done | bytes 81944
  6.1 0.0 copy-start.6
  6.1 0.9 %copy-done.6 = bf16[1280,32]{0,1:T(8,128)(2,1)S(1)} copy-done((bf16[1280,32]{0,1:T(8,128)(2,1)S(1)}, bf16[1280,32]{0,1:T(8,128)(2,1)}, u32[]{:S(2)}) %copy-start.6) | copy-done | bytes 81944
  7.0 0.7 copy-done.9
  7.7 0.7 copy-done.11
  8.4 75.5 %shard_map.118 = bf16[256,512]{1,0:T(8,128)(2,1)S(1)} custom-call(bf16[256,512]{1,0:T(8,128)(2,1)S(1)} %bitcast.12, f32[1,1024]{1,0:T(1,128)S(1)} %bitcast.16, bf16[32,1280]{1,0:T(8,128)(2,1)S(1)} %copy-done.1, bf16[32,1280]{1,0:T(8,128)(2,1)S(1)} %copy-done.2, bf16[32,1280]{1,0:T(8,128)(2,1)S(1)} %bitcast.13, f32[1,512]{1,0:T(1,128)S(1)} %bitcast.18, ...), custom_call_target="tpu_custom_call" | custom-call | tf_op jit(solution)/shard_map/pallas_call | solution.py:484
  83.9 0.7 copy.14
  (2 shorter events, 0.0 us)
Async XLA Ops:
  0.0 0.7 copy-start.7
  0.0 0.7 copy-start.8
  0.0 0.7 copy-start.10
  0.7 0.9 %copy-start = (bf16[1,256,512]{2,1,0:T(8,128)(2,1)S(1)}, bf16[1,256,512]{2,1,0:T(8,128)(2,1)}, u32[]{:S(2)}) copy-start(bf16[1,256,512]{2,1,0:T(8,128)(2,1)} %param.12) | copy-start | bytes 786436
  1.7 0.9 %copy-start.1 = (bf16[32,1280]{1,0:T(8,128)(2,1)S(1)}, bf16[32,1280]{1,0:T(8,128)(2,1)}, u32[]{:S(2)}) copy-start(bf16[32,1280]{1,0:T(8,128)(2,1)} %gate1.1) | copy-start | bytes 245764
  2.6 0.9 %copy-start.2 = (bf16[32,1280]{1,0:T(8,128)(2,1)S(1)}, bf16[32,1280]{1,0:T(8,128)(2,1)}, u32[]{:S(2)}) copy-start(bf16[32,1280]{1,0:T(8,128)(2,1)} %up1.1) | copy-start | bytes 245764
  3.4 0.9 %copy-start.3 = (bf16[1280,32]{0,1:T(8,128)(2,1)S(1)}, bf16[1280,32]{0,1:T(8,128)(2,1)}, u32[]{:S(2)}) copy-start(bf16[1280,32]{0,1:T(8,128)(2,1)} %param.16) | copy-start | bytes 245764
  4.3 0.9 %copy-start.4 = (bf16[32,1280]{1,0:T(8,128)(2,1)S(1)}, bf16[32,1280]{1,0:T(8,128)(2,1)}, u32[]{:S(2)}) copy-start(bf16[32,1280]{1,0:T(8,128)(2,1)} %gate2.1) | copy-start | bytes 245764
  5.2 0.9 %copy-start.5 = (bf16[32,1280]{1,0:T(8,128)(2,1)S(1)}, bf16[32,1280]{1,0:T(8,128)(2,1)}, u32[]{:S(2)}) copy-start(bf16[32,1280]{1,0:T(8,128)(2,1)} %up2.1) | copy-start | bytes 245764
  6.1 0.9 %copy-start.6 = (bf16[1280,32]{0,1:T(8,128)(2,1)S(1)}, bf16[1280,32]{0,1:T(8,128)(2,1)}, u32[]{:S(2)}) copy-start(bf16[1280,32]{0,1:T(8,128)(2,1)} %param.23) | copy-start | bytes 245764
  7.0 0.7 copy-start.9
  7.7 0.7 copy-start.11

commit v2 on v1

--- a/solution.py
+++ b/solution.py
@@ -514,7 +514,7 @@
             pltpu.SemaphoreType.DMA((N_RECV,)),
             pltpu.SemaphoreType.DMA((N_LOCAL,)),
         ],
-        compiler_params=pltpu.CompilerParams(collective_id=0, has_side_effects=True, vmem_limit_bytes=48 * 2**20),
+        compiler_params=pltpu.CompilerParams(collective_id=0, has_side_effects=True, vmem_limit_bytes=67043328),
     )(
         tok.reshape(256, HALF), g1.reshape(1, D), gate1, up1, down1.T, mixg.reshape(1, HALF),
         pool.transpose(0, 2, 1).reshape(16, 256), scale.reshape(1, HALF), g2.reshape(1, D), gate2, up2, down2.T,

time: 85 us -> 78.8 us (0.927)
  local copies, waits for them, and re-layouts: 9.05 us -> 1.67 us
  Pallas kernels: 75.5 us -> 76.9 us
    unnamed x25 -> x1, local copies, waits for them, and re-layouts: 9.05 us -> 1.67 us
    pallas_call x1, Pallas kernels: 75.5 us -> 76.9 us  [local(): pl.pallas_call(kernel, out_shape=jax.ShapeDtypeStruct((256, HALF), BF16),...]
where the time goes in v2:
time: 78.8 us; the launch traced here: 78.6 us
  Pallas kernels  76.9 us (98%)
  local copies, waits for them, and re-layouts  1.67 us (2%)
    pallas_call x1, Pallas kernels, local(): pl.pallas_call(kernel, out_shape=jax.ShapeDtypeStruct((256, HALF), BF16),...  76.9 us
    unnamed x1, local copies, waits for them, and re-layouts  1.67 us

profile of v2, /device:TPU:1, one launch (start us, length us, event | category | flops | bytes accessed | tf_op | source)
XLA Modules:
  0.0 78.6 jit_solution(13411381067853745838)
XLA Ops:
  0.0 76.9 %shard_map.118 = bf16[256,512]{1,0:T(8,128)(2,1)} custom-call(bf16[256,512]{1,0:T(8,128)(2,1)} %bitcast.12, f32[1,1024]{1,0:T(1,128)} %bitcast.16, bf16[32,1280]{1,0:T(8,128)(2,1)} %gate1.1, bf16[32,1280]{1,0:T(8,128)(2,1)} %up1.1, bf16[32,1280]{1,0:T(8,128)(2,1)} %bitcast.13, f32[1,512]{1,0:T(1,128)} %bitcast.18, bf16[16,256]{1,0:T(8,128)(2,1)} %bitcast.15, ...), custom_call_target="tpu_custom_call" | custom-call | tf_op jit(solution)/shard_map/pallas_call | solution.py:484
  76.9 1.7 %copy.14 = bf16[1,256,512]{2,1,0:T(8,128)(2,1)} copy(bf16[1,256,512]{2,1,0:T(8,128)(2,1)} %bitcast.11) | data formatting | bytes 524288

commit v3 on v2

v3 whole, which is shorter than its diff:
```python
import jax
import jax.numpy as jnp
from jax import lax
from jax.experimental import pallas as pl
from jax.experimental.pallas import tpu as pltpu
from jax.sharding import PartitionSpec as P

MESH = pl.DeviceIdType.MESH
BF16 = jnp.bfloat16
F32 = jnp.float32
EPS = 1e-06
D = 1024
HALF = 512
ROWS = 128
UNIT = 640
N_SEND = 35
N_RECV = 98
N_LOCAL = 7


class Net:
    def __init__(self, ss, rs, ls, here):
        self.ss, self.rs, self.ls, self.here = ss, rs, ls, here
        self.names = {}
        self.batches = {}
        self.locals = 0
        self.sends = 0
        self.pending = []

    def name(self, key, width=1):
        if key not in self.names:
            self.names[key] = sum(w for _, w in self.names.values()), width
        return self.names[key][0]

    def send(self, key, make, cond=None, width=1, shift=None, batch=None, total=None):
        base = self.name(key, width)
        first = batch is None or batch not in self.batches
        if first:
            slot = self.sends
            self.sends += 1
            if batch is not None:
                self.batches[batch] = slot
        else:
            slot = self.batches[batch]

        def copy(src, dst, device):
            where = base if shift is None else base + shift
            return pltpu.make_async_remote_copy(
                src, dst, self.ss.at[slot], self.rs.at[where], device_id=device, device_id_type=MESH
            )

        def end():
            ref = make()[0] if total is None else total()
            copy(ref, ref, self.here).wait_send()

        if cond is None:
            copy(*make()).start()
        else:
            pl.when(cond)(lambda: copy(*make()).start())
        if first:
            self.pending.append(end if cond is None else lambda: pl.when(cond)(end))

    def recv(self, key, ref, offset=0, width=1):
        where = self.name(key, width) + offset
        pltpu.make_async_remote_copy(
            ref, ref, self.ss.at[0], self.rs.at[where], device_id=self.here, device_id_type=MESH
        ).wait_recv()

    def slot(self):
        self.locals += 1
        return self.ls.at[self.locals - 1]

    def local(self, src, dst):
        return pltpu.make_async_copy(src, dst, self.slot())

    def finish(self):
        for end in self.pending:
            end()
        assert self.sends == N_SEND and self.locals == N_LOCAL
        assert sum(w for _, w in self.names.values()) == N_RECV


class Stream:
    def __init__(self, net, unit, tag, direct, piece, group, size, many, first, second, sibling):
        self.net, self.unit, self.tag, self.direct = net, unit, (unit, tag), direct
        self.piece, self.group, self.size, self.many = piece, group, size, many
        self.a, self.ap, self.am, self.ao, self.to_ap, self.to_am, self.to_ao = first
        self.b, self.bp, self.bm, self.bo, self.to_bp, self.to_bm, self.to_bo = second
        self.sibling = sibling

    def send(self, what, a, b, device, kind, count):
        self.net.send(
            (self.tag, what),
            lambda: (self.piece(a, b), self.piece(a, b), device),
            batch=(self.unit, kind),
            total=lambda: self.size(count * self.many),
        )

    def recv(self, what, a, b):
        self.net.recv((self.tag, what), self.piece(a, b))

    def both(self, k, a):
        late_m, late_p = ("2m23" if k >= 2 else f"2m{k}"), ("2p01" if k < 2 else f"2p{k}")
        self.send(late_m, a, self.b, self.to_bp, "both", 8)
        self.send(late_p, a, self.b, self.to_bm, "both", 8)

    def hand(self, b):
        self.net.send(
            (self.unit, "d"),
            lambda: (self.group(b), self.group(b), self.sibling),
            batch=(self.unit, "hand"),
            total=lambda: self.size(16 * self.many),
        )

    def one(self):
        self.send("1m", self.a, self.b, self.to_ap, "ring", 2)
        self.send("1p", self.a, self.b, self.to_am, "ring", 2)
        if self.direct:
            self.send("1o", self.a, self.b, self.to_ao, "far", 1)

    def then(self):
        self.both(0, self.a)

    def two(self):
        self.recv("1m", self.am, self.b)
        if not self.direct:
            self.send("1o", self.am, self.b, self.to_ap, "far", 1)
        self.both(1, self.am)
        self.recv("1p", self.ap, self.b)
        self.both(2, self.ap)

    def three(self):
        self.recv("1o", self.ao, self.b)
        self.both(3, self.ao)
        self.hand(self.b)

    def four(self):
        self.recv("2m0", self.a, self.bm)
        self.send("2o", self.a, self.bm, self.to_bp, "on", 4)
        self.recv("2m1", self.am, self.bm)
        self.send("2o", self.am, self.bm, self.to_bp, "on", 4)
        self.recv("2p2", self.ap, self.bp)
        self.send("2o", self.ap, self.bp, self.to_bm, "on", 4)
        self.recv("2p3", self.ao, self.bp)
        self.send("2o", self.ao, self.bp, self.to_bm, "on", 4)
        self.net.recv((self.tag, "2p01"), self.size(2))
        self.hand(self.bp)
        self.net.recv((self.tag, "2m23"), self.size(2))
        self.hand(self.bm)

    def five(self):
        self.net.recv((self.tag, "2o"), self.size(4))
        self.hand(self.bo)


def normed(values, gain):
    floats = values.astype(F32)
    mean = jnp.mean(floats * floats, axis=-1, keepdims=True)
    return (floats * lax.rsqrt(mean + EPS) * gain).astype(BF16)


def kernel(
    tok, g1, gate1, up1, down1, mixg, pool, scale, g2, gate2, up2, down2, out,
    w, pw, xt, xq, n, h1, h2, wd1, wd2, maps, own1, pm, pp, so, sm, sp, ra, rb, a1, hs, hr, mg, ob, sq, rq, base, rx,
    ss, rs, ls,
):
    rep = lax.axis_index("rep")
    fs = lax.axis_index("fs")
    c = lax.axis_index("tp")
    o = 1 - c
    j = lax.div(fs, 16)
    z = rep * 2 + j
    y = lax.rem(lax.div(fs, 4), 4)
    x = lax.rem(fs, 4)
    zp, zo, zm = (lax.rem(z + k, 4) for k in (1, 2, 3))
    yp, yo, ym = (lax.rem(y + k, 4) for k in (1, 2, 3))
    xp, xo, xm = (lax.rem(x + k, 4) for k in (1, 2, 3))

    def dev(z_, y_, x_, c_):
        return (lax.div(z_, 2), lax.rem(z_, 2) * 16 + y_ * 4 + x_, c_)

    sibling = dev(z, y, x, o)
    net = Net(ss, rs, ls, sibling)
    keeper = c == j
    taker = c != j
    zq = lax.rem(z + 1 + 2 * lax.rem(z + c, 2), 4)

    def cols(k):
        return pl.ds(pl.multiple_of(k * UNIT, 128), UNIT)

    def feats(k):
        return pl.ds(pl.multiple_of(k * HALF, 128), HALF)

    def rows(k):
        return pl.ds(pl.multiple_of(k * ROWS, 128), ROWS)

    mats = ((gate1, up1, down1), (gate2, up2, down2), (gate2, up2, down2))
    subs = (lax.div(z, 2), 0, 1)

    own_tok = net.local(tok.at[rows(c), :], xt.at[z, :, feats(c)])
    own_tok.start()
    own_w = [net.slot() for u in range(3)]
    own_p = net.slot()

    def own_pool():
        return pltpu.make_async_copy(pool, pw.at[c, c, y, x], own_p)

    @pl.when(keeper)
    def _():
        for u in range(3):
            for m in range(3):
                pltpu.make_async_copy(mats[u][m].at[:, cols(subs[u])], w.at[u, m, c, y, x], own_w[u]).start()
        own_pool().start()

    own_mg = net.local(mixg, mg.at[0, c])
    own_sc = net.local(scale, mg.at[1, c])
    own_mg.start()
    own_sc.start()

    barrier = pltpu.get_barrier_semaphore()
    friends = [dev(z, y, x_, c) for x_ in (xp, xm, xo)] + [dev(z, y_, x, c) for y_ in (yp, ym, yo)] + [sibling]
    friends += [dev(z_, y, x, k) for z_ in (zp, zm) for k in range(2)]
    for friend in friends:
        pl.semaphore_signal(barrier, inc=1, device_id=friend, device_id_type=MESH)
    pl.semaphore_wait(barrier, len(friends))

    def exchange(u):
        for ab, z_ in ((0, zp), (1, zm)):
            sub = (lax.div(z_, 2), 0, 1)[u]
            part = pl.ds(16 * ab, 16)
            for m in range(3):
                net.send(
                    ("z", u),
                    lambda m=m, part=part, sub=sub, z_=z_: (
                        mats[u][m].at[part, cols(sub)],
                        w.at[u, m, o, y, x, part, :],
                        dev(z_, y, x, o),
                    ),
                    cond=taker,
                    batch=("z", u),
                    total=lambda: w.at[u, :, 0, 0, 0],
                )

    def own(u):
        ref = w.at[u, :, c, y, x]

        @pl.when(keeper)
        def _():
            pltpu.make_async_copy(ref, ref, own_w[u]).wait()

        @pl.when(taker)
        def _():
            net.recv(("z", u), ref)

    in_x = (x, xp, xm, xo, dev(z, y, xp, c), dev(z, y, xm, c), dev(z, y, xo, c))
    in_y = (y, yp, ym, yo, dev(z, yp, x, c), dev(z, ym, x, c), dev(z, yo, x, c))
    two, top, low = pl.ds(0, 2), pl.ds(0, 16), pl.ds(16, 16)

    def size_w(k):
        return {
            2: w.at[0, :, 0, two, 0, top],
            4: w.at[0, :, 0, :, 0, top],
            8: w.at[0, :, 0, two, :, top],
            16: w.at[0, :, 0, :, :, top],
            32: w.at[0, :, 0],
        }[k]

    def size_p(k):
        return {1: pw.at[:, 0, 0, 0], 2: pw.at[:, 0, two, 0], 4: pw.at[:, 0, 0], 8: pw.at[:, 0, two], 16: pw.at[:, 0]}[k]

    def stream_a(u):
        return Stream(
            net, u, "a", u == 0,
            lambda a, b: w.at[u, :, c, b, a, top, :],
            lambda b: w.at[u, :, c, b, :, top, :],
            size_w, 2, in_x, in_y, sibling,
        )

    def stream_b(u):
        return Stream(
            net, u, "b", u == 0,
            lambda a, b: w.at[u, :, c, a, b, low, :],
            lambda b: w.at[u, :, c, :, b, low, :],
            size_w, 2, in_y, in_x, sibling,
        )

    sa = [stream_a(u) for u in range(3)]
    sb = [stream_b(u) for u in range(3)]
    spool = Stream(
        net, "p", "a", False, lambda a, b: pw.at[:, c, b, a], lambda b: pw.at[:, c, b], size_p, 1, in_x, in_y, sibling
    )

    def start(u):
        own(u)
        sa[u].one()
        sb[u].one()
        sa[u].then()
        sb[u].then()

    def handed(u):
        net.recv((u, "d"), w.at[u, :, o])

    def spread_tokens():
        for k in range(2):
            for key, z_ in (("tm", zp), ("tp", zm)):
                net.send(
                    key,
                    lambda k=k, z_=z_: (tok.at[rows(k), :], xt.at[z, :, feats(c)], dev(z_, y, x, k)),
                    width=2, shift=c, batch="t4", total=lambda: xt.at[pl.ds(0, 2)],
                )
        net.send("ts", lambda: (tok.at[rows(o), :], xt.at[z, :, feats(c)], sibling))

    def relay_tokens():
        for key, who, half, to in (("tm", zm, 0, zp), ("tp", zp, 1, zm)):
            net.recv(key, xt.at[who, :, feats(half)], half, 2)
            net.send(
                "to",
                lambda who=who, half=half, to=to: (
                    xt.at[who, :, feats(half)], xt.at[who, :, feats(half)], dev(to, y, x, c)
                ),
                batch="t2", total=lambda: xt.at[0],
            )
        net.recv("tm", xt.at[zm, :, feats(1)], 1, 2)
        net.recv("tp", xt.at[zp, :, feats(0)], 0, 2)

    def gate_up(u, at, count, put):
        for k in range(UNIT // 128):
            part = pl.ds(k * 128, 128)
            wg = w[u, 0, :, :, :, :, part].reshape(D, 128)
            wu = w[u, 1, :, :, :, :, part].reshape(D, 128)
            both = jnp.dot(
                n[pl.ds(at, count), :], jnp.concatenate([wg, wu], axis=1), preferred_element_type=F32
            )
            gate, up = both[:, :128], both[:, 128:]
            put(k * 128, (gate * jax.nn.sigmoid(gate) * up).astype(BF16))

    def put1(at, count):
        def put(k, value):
            h1[pl.ds(at, count), pl.ds(k, 128)] = value

        return put

    def put2(at, count, first):
        def put(k, value):
            h2[pl.ds(at, count), pl.ds(first + k, 128)] = value

        return put

    def turn(u, part, wide, at):
        for k in range(2):
            block = w[u, 2, part, 2 * k : 2 * k + 2].reshape(256, UNIT)
            wide[pl.ds(at, UNIT), pl.ds(pl.multiple_of(part * HALF + 256 * k, 128), 256)] = block.T

    def dot(lhs, rhs):
        return jnp.dot(lhs, rhs, preferred_element_type=F32)

    exchange(0)
    spread_tokens()
    start(0)
    exchange(1)
    exchange(2)
    net.send("ps", lambda: (pool, pw.at[c, o, y, x], sibling), cond=taker)
    net.send("pz", lambda: (pool, pw.at[c, j, y, x], dev(zp, y, x, j)), width=2, shift=c)
    own_mg.wait()
    own_sc.wait()
    net.send("mg", lambda: (mixg, mg.at[0, c], sibling), batch="mg", total=lambda: mg.at[:, 0])
    net.send("mg", lambda: (scale, mg.at[1, c], sibling), batch="mg", total=lambda: mg.at[:, 0])

    sa[0].two()
    sb[0].two()
    gain1 = g1[...]
    own_tok.wait()
    net.recv("ts", xt.at[z, :, feats(o)])
    n[pl.ds(0, ROWS), :] = normed(xt[z], gain1)
    sa[0].three()
    sb[0].three()
    relay_tokens()
    sa[0].four()
    sb[0].four()
    start(1)

    @pl.when(keeper)
    def _():
        own_pool().wait()
        net.recv("ps", pw.at[o, c, y, x])

    @pl.when(taker)
    def _():
        net.recv("pz", pw.at[0, c, y, x], 0, 2)
        net.recv("pz", pw.at[1, c, y, x], 1, 2)

    spool.one()
    spool.then()
    start(2)
    n[pl.ds(ROWS, ROWS), :] = normed(xt[zm], gain1)
    n[pl.ds(2 * ROWS, ROWS), :] = normed(xt[zp], gain1)
    net.recv("to", xt.at[zo])
    n[pl.ds(3 * ROWS, ROWS), :] = normed(xt[zo], gain1)
    sa[0].five()
    sb[0].five()
    turn(0, c, wd1, 0)
    handed(0)

    gate_up(0, 3 * ROWS, ROWS, put1(3 * ROWS, ROWS))
    turn(0, o, wd1, 0)
    so[...] = dot(h1[pl.ds(3 * ROWS, ROWS), :], wd1[...]).astype(BF16)
    net.send("r0", lambda: (so.at[:, feats(0)], ra.at[0], dev(zp, y, x, c)), batch="r", total=lambda: so)
    net.send("r1", lambda: (so.at[:, feats(1)], ra.at[1], dev(zm, y, x, c)), batch="r", total=lambda: so)
    sa[1].two()
    sb[1].two()
    spool.two()
    gate_up(0, ROWS, 2 * ROWS, put1(ROWS, 2 * ROWS))
    sums = dot(h1[pl.ds(ROWS, 2 * ROWS), :], wd1[...])
    sm[:, :HALF] = sums[:ROWS, :HALF].astype(BF16)
    sp[:, HALF:] = sums[ROWS:, HALF:].astype(BF16)
    pm[...] = sums[:ROWS, HALF:]
    pp[...] = sums[ROWS:, :HALF]

    def pass_on(key, buf, k, half, z_):
        net.send(
            f"{key}{half}",
            lambda: (buf.at[:, feats(half)], rb.at[k, :, feats(half)], dev(z_, y, x, c)),
            batch="q", total=lambda: xt.at[two],
        )

    pass_on("qm", sp, 0, 1, zp)
    pass_on("qp", sm, 1, 0, zm)
    sa[1].three()
    sb[1].three()
    spool.three()
    gate_up(0, 0, ROWS, put1(0, ROWS))
    own1[...] = dot(h1[pl.ds(0, ROWS), :], wd1[...])
    net.recv("r0", ra.at[0])
    sp[:, :HALF] = (pp[...] + ra[0].astype(F32)).astype(BF16)
    net.recv("r1", ra.at[1])
    sm[:, HALF:] = (pm[...] + ra[1].astype(F32)).astype(BF16)
    pass_on("qm", sp, 0, 0, zp)
    pass_on("qp", sm, 1, 1, zm)
    sa[2].two()
    sb[2].two()
    sa[1].four()
    sb[1].four()
    spool.four()
    sa[2].three()
    sb[2].three()
    spool.five()
    net.recv(("p", "d"), pw.at[:, o])
    for g in range(4):
        wide = pw[g // 2].reshape(32, 16, 256).astype(F32)
        maps[g] = wide[:, 8 * (g % 2) : 8 * (g % 2) + 8, :].reshape(256, 256).astype(BF16).T
    sa[1].five()
    sb[1].five()
    turn(1, c, wd2, 0)
    for key, k, half in (("qm", 0, 1), ("qp", 1, 0), ("qm", 0, 0), ("qp", 1, 1)):
        net.recv(f"{key}{half}", rb.at[k, :, feats(half)])
    block = own1[...] + rb[0].astype(F32) + rb[1].astype(F32)
    a1[...] = (xt[z].astype(F32) + 0.5 * block).astype(BF16)

    net.recv("mg", mg.at[:, o])
    mix_gain = jnp.concatenate([mg[0, 0], mg[0, 1]], axis=1)
    mix_scale = jnp.concatenate([mg[1, 0], mg[1, 1]], axis=1)
    hidden = normed(a1[...], mix_gain)
    hs[...] = hidden
    net.send("h", lambda: (hs.at[pl.ds(112, 16), :], hr, sibling))
    net.recv("h", hr)
    before = jnp.where(c == 1, hr[...].astype(F32), 0.0)
    floats = hs[...].astype(F32)
    longer = jnp.concatenate([before, floats], axis=0)
    positions = c * ROWS + lax.broadcasted_iota(jnp.int32, (ROWS, 256), 0)
    for g in range(4):
        lanes = slice(256 * g, 256 * g + 256)
        total = longer[:, lanes]
        for k in range(g + 1):
            total = total + pltpu.roll(total, 2**k, axis=0)
        counts = jnp.minimum(positions + 1, 2 ** (g + 1)).astype(F32)
        diff = (total[16:] / counts - floats[:, lanes]).astype(BF16)
        mixed = dot(diff, maps[g])
        after = a1[:, lanes].astype(F32) + mixed * mix_scale[:, lanes]
        ob[:, lanes] = after.astype(BF16)

    net.send("a", lambda: (ob, xq, dev(zq, y, x, c)))
    gain2 = g2[...]
    n[pl.ds(0, ROWS), :] = normed(ob[...], gain2)
    sa[2].four()
    sb[2].four()
    handed(1)
    gate_up(1, 0, ROWS, put2(0, ROWS, 0))
    turn(1, o, wd2, 0)
    sa[2].five()
    sb[2].five()
    turn(2, c, wd2, UNIT)
    net.recv("a", xq)
    n[pl.ds(ROWS, ROWS), :] = normed(xq[...], gain2)
    gate_up(1, ROWS, ROWS, put2(ROWS, ROWS, 0))
    handed(2)
    gate_up(2, ROWS, ROWS, put2(ROWS, ROWS, UNIT))
    turn(2, o, wd2, UNIT)
    sq[...] = dot(h2[pl.ds(ROWS, ROWS), :], wd2[...]).astype(BF16)
    for k in range(2):
        net.send(
            "b",
            lambda k=k: (sq.at[:, feats(k)], rq.at[c], dev(zq, y, x, k)),
            width=2, shift=c, batch="b", total=lambda: sq,
        )
    gate_up(2, 0, ROWS, put2(0, ROWS, UNIT))
    base[...] = ob[...].astype(F32) + 0.5 * dot(h2[pl.ds(0, ROWS), :], wd2[...])
    net.send("f", lambda: (base.at[:, feats(o)], rx, sibling))
    net.recv("b", rq.at[c], c, 2)
    out[rows(c), :] = (base[:, feats(c)] + 0.5 * rq[c].astype(F32)).astype(BF16)
    net.recv("f", rx)
    net.recv("b", rq.at[o], o, 2)
    out[rows(o), :] = (rx[...] + 0.5 * rq[o].astype(F32)).astype(BF16)
    net.finish()


def local(tok, g1, gate1, up1, down1, mixg, pool, scale, g2, gate2, up2, down2):
    hbm = pl.BlockSpec(memory_space=pl.ANY)
    vmem = pl.BlockSpec(memory_space=pltpu.VMEM)
    result = pl.pallas_call(
        kernel,
        out_shape=jax.ShapeDtypeStruct((256, HALF), BF16),
        in_specs=[hbm, vmem, hbm, hbm, hbm, hbm, hbm, hbm, vmem, hbm, hbm, hbm],
        out_specs=vmem,
        scratch_shapes=[
            pltpu.VMEM((3, 3, 2, 4, 4, 32, UNIT), BF16),
            pltpu.VMEM((2, 2, 4, 4, 16, 256), BF16),
            pltpu.VMEM((4, ROWS, D), BF16),
            pltpu.VMEM((ROWS, D), BF16),
            pltpu.VMEM((4 * ROWS, D), BF16),
            pltpu.VMEM((4 * ROWS, UNIT), BF16),
            pltpu.VMEM((2 * ROWS, 2 * UNIT), BF16),
            pltpu.VMEM((UNIT, D), BF16),
            pltpu.VMEM((2 * UNIT, D), BF16),
            pltpu.VMEM((4, 256, 256), BF16),
            pltpu.VMEM((ROWS, D), F32),
            pltpu.VMEM((ROWS, HALF), F32),
            pltpu.VMEM((ROWS, HALF), F32),
            pltpu.VMEM((ROWS, D), BF16),
            pltpu.VMEM((ROWS, D), BF16),
            pltpu.VMEM((ROWS, D), BF16),
            pltpu.VMEM((2, ROWS, HALF), BF16),
            pltpu.VMEM((2, ROWS, D), BF16),
            pltpu.VMEM((ROWS, D), BF16),
            pltpu.VMEM((ROWS, D), BF16),
            pltpu.VMEM((16, D), BF16),
            pltpu.VMEM((2, 2, 1, HALF), F32),
            pltpu.VMEM((ROWS, D), BF16),
            pltpu.VMEM((ROWS, D), BF16),
            pltpu.VMEM((2, ROWS, HALF), BF16),
            pltpu.VMEM((ROWS, D), F32),
            pltpu.VMEM((ROWS, HALF), F32),
            pltpu.SemaphoreType.DMA((N_SEND,)),
            pltpu.SemaphoreType.DMA((N_RECV,)),
            pltpu.SemaphoreType.DMA((N_LOCAL,)),
        ],
        compiler_params=pltpu.CompilerParams(collective_id=0, has_side_effects=True, vmem_limit_bytes=67043328),
    )(
        tok.reshape(256, HALF), g1.reshape(1, D), gate1, up1, down1.T, mixg.reshape(1, HALF),
        pool.transpose(0, 2, 1).reshape(16, 256), scale.reshape(1, HALF), g2.reshape(1, D), gate2, up2, down2.T,
    )
    return result.reshape(1, 256, HALF)


def solution(mesh):
    placed = (
        P(("rep", "fs"), None, "tp"),
        P(),
        P("fs", "tp"),
        P("fs", "tp"),
        P("tp", "fs"),
        P("tp"),
        P("tp", None, "fs"),
        P("tp"),
        P(),
        P("fs", "tp"),
        P("fs", "tp"),
        P("tp", "fs"),
    )
    return jax.shard_map(
        local, mesh=mesh, in_specs=placed, out_specs=P(("rep", "fs"), None, "tp"), check_vma=False
    )
```

time: 78.8 us -> 67.1 us (0.85)
  Pallas kernels: 76.9 us -> 65.2 us
    pallas_call x1, Pallas kernels: 76.9 us -> 65.2 us  [local(): pl.pallas_call(kernel, out_shape=jax.ShapeDtypeStruct((256, HALF), BF16),...]
where the time goes in v3:
time: 67.1 us; the launch traced here: 66.9 us
  Pallas kernels  65.2 us (97%)
  local copies, waits for them, and re-layouts  1.67 us (2%)
    pallas_call x1, Pallas kernels, local(): pl.pallas_call(kernel, out_shape=jax.ShapeDtypeStruct((256, HALF), BF16),...  65.2 us
    unnamed x1, local copies, waits for them, and re-layouts  1.67 us

profile of v3, /device:TPU:1, one launch (start us, length us, event | category | flops | bytes accessed | tf_op | source)
XLA Modules:
  0.0 66.9 jit_solution(17610422192566776843)
XLA Ops:
  0.0 65.2 %shard_map.118 = bf16[256,512]{1,0:T(8,128)(2,1)} custom-call(bf16[256,512]{1,0:T(8,128)(2,1)} %bitcast.12, f32[1,1024]{1,0:T(1,128)} %bitcast.16, bf16[32,1280]{1,0:T(8,128)(2,1)} %gate1.1, bf16[32,1280]{1,0:T(8,128)(2,1)} %up1.1, bf16[32,1280]{1,0:T(8,128)(2,1)} %bitcast.13, f32[1,512]{1,0:T(1,128)} %bitcast.18, bf16[16,256]{1,0:T(8,128)(2,1)} %bitcast.15, ...), custom_call_target="tpu_custom_call" | custom-call | tf_op jit(solution)/shard_map/pallas_call | solution.py:519
  65.3 1.7 %copy.14 = bf16[1,256,512]{2,1,0:T(8,128)(2,1)} copy(bf16[1,256,512]{2,1,0:T(8,128)(2,1)} %bitcast.11) | data formatting | bytes 524288

commit v4 on v3

--- a/solution.py
+++ b/solution.py
@@ -13,9 +13,10 @@
 HALF = 512
 ROWS = 128
 UNIT = 640
+DIRECT = True
 N_SEND = 35
-N_RECV = 98
-N_LOCAL = 7
+N_RECV = 90
+N_LOCAL = 10
 
 
 class Net:
@@ -134,9 +135,11 @@
         self.both(3, self.ao)
         self.hand(self.b)
 
-    def four(self):
+    def pre(self):
         self.recv("2m0", self.a, self.bm)
         self.send("2o", self.a, self.bm, self.to_bp, "on", 4)
+
+    def four(self):
         self.recv("2m1", self.am, self.bm)
         self.send("2o", self.am, self.bm, self.to_bp, "on", 4)
         self.recv("2p2", self.ap, self.bp)
@@ -153,6 +156,31 @@
         self.hand(self.bo)
 
 
+class Coarse:
+    def __init__(self, net, buf, c, y, x, to_row, to_column, sibling):
+        self.net, self.buf, self.c, self.y, self.x = net, buf, c, y, x
+        self.to_row, self.to_column, self.sibling = to_row, to_column, sibling
+
+    def send(self, key, make, device, size):
+        self.net.send(key, lambda: (make(), make(), device), batch=key, total=lambda: size)
+
+    def first(self):
+        for device in self.to_row:
+            self.send("p1", lambda: self.buf.at[:, self.c, self.y, self.x], device, self.buf.at[:, 0, 0, pl.ds(0, 3)])
+
+    def second(self):
+        self.net.recv("p1", self.buf.at[:, 0, 0, pl.ds(0, 3)])
+        for device in self.to_column:
+            self.send("p2", lambda: self.buf.at[:, self.c, self.y], device, self.buf.at[:, 0, pl.ds(0, 3)])
+
+    def third(self):
+        self.net.recv("p2", self.buf.at[:, 0, pl.ds(0, 3)])
+        self.send("p3", lambda: self.buf.at[:, self.c], self.sibling, self.buf.at[:, 0])
+
+    def last(self, o):
+        self.net.recv("p3", self.buf.at[:, o])
+
+
 def normed(values, gain):
     floats = values.astype(F32)
     mean = jnp.mean(floats * floats, axis=-1, keepdims=True)
@@ -161,7 +189,7 @@
 
 def kernel(
     tok, g1, gate1, up1, down1, mixg, pool, scale, g2, gate2, up2, down2, out,
-    w, pw, xt, xq, n, h1, h2, wd1, wd2, maps, own1, pm, pp, so, sm, sp, ra, rb, a1, hs, hr, mg, ob, sq, rq, base, rx,
+    w, pw, xt, xq, n, h1, h2, wd1, wd2, maps, own1, pm, pp, so, sm, sp, ra, rb, a1, hs, hr, mg, ob, sq, rq, base, rx, st, tokv,
     ss, rs, ls,
 ):
     rep = lax.axis_index("rep")
@@ -205,6 +233,16 @@
     def own_pool():
         return pltpu.make_async_copy(pool, pw.at[c, c, y, x], own_p)
 
+    stage_t = net.local(tok, tokv)
+    stage_t.start()
+    stage_w = [net.slot(), net.slot()]
+
+    @pl.when(taker)
+    def _():
+        for k in range(2):
+            for m in range(3):
+                pltpu.make_async_copy(mats[k][m], st.at[k, m], stage_w[k]).start()
+
     @pl.when(keeper)
     def _():
         for u in range(3):
@@ -223,6 +261,11 @@
     for friend in friends:
         pl.semaphore_signal(barrier, inc=1, device_id=friend, device_id_type=MESH)
     pl.semaphore_wait(barrier, len(friends))
+
+    def staged(k):
+        @pl.when(taker)
+        def _():
+            pltpu.make_async_copy(st.at[k], st.at[k], stage_w[k]).wait()
 
     def exchange(u):
         for ab, z_ in ((0, zp), (1, zm)):
@@ -232,7 +275,7 @@
                 net.send(
                     ("z", u),
                     lambda m=m, part=part, sub=sub, z_=z_: (
-                        mats[u][m].at[part, cols(sub)],
+                        st.at[min(u, 1), m, part, cols(sub)],
                         w.at[u, m, o, y, x, part, :],
                         dev(z_, y, x, o),
                     ),
@@ -265,12 +308,9 @@
             32: w.at[0, :, 0],
         }[k]
 
-    def size_p(k):
-        return {1: pw.at[:, 0, 0, 0], 2: pw.at[:, 0, two, 0], 4: pw.at[:, 0, 0], 8: pw.at[:, 0, two], 16: pw.at[:, 0]}[k]
-
     def stream_a(u):
         return Stream(
-            net, u, "a", u == 0,
+            net, u, "a", DIRECT and u == 0,
             lambda a, b: w.at[u, :, c, b, a, top, :],
             lambda b: w.at[u, :, c, b, :, top, :],
             size_w, 2, in_x, in_y, sibling,
@@ -278,7 +318,7 @@
 
     def stream_b(u):
         return Stream(
-            net, u, "b", u == 0,
+            net, u, "b", DIRECT and u == 0,
             lambda a, b: w.at[u, :, c, a, b, low, :],
             lambda b: w.at[u, :, c, :, b, low, :],
             size_w, 2, in_y, in_x, sibling,
@@ -286,9 +326,7 @@
 
     sa = [stream_a(u) for u in range(3)]
     sb = [stream_b(u) for u in range(3)]
-    spool = Stream(
-        net, "p", "a", False, lambda a, b: pw.at[:, c, b, a], lambda b: pw.at[:, c, b], size_p, 1, in_x, in_y, sibling
-    )
+    spool = Coarse(net, pw, c, y, x, (in_x[4], in_x[5], in_x[6]), (in_y[4], in_y[5], in_y[6]), sibling)
 
     def start(u):
         own(u)
@@ -300,15 +338,15 @@
     def handed(u):
         net.recv((u, "d"), w.at[u, :, o])
 
-    def spread_tokens():
+    def spread_tokens(tag, cond):
         for k in range(2):
             for key, z_ in (("tm", zp), ("tp", zm)):
                 net.send(
                     key,
-                    lambda k=k, z_=z_: (tok.at[rows(k), :], xt.at[z, :, feats(c)], dev(z_, y, x, k)),
-                    width=2, shift=c, batch="t4", total=lambda: xt.at[pl.ds(0, 2)],
+                    lambda k=k, z_=z_: (tokv.at[rows(k), :], xt.at[z, :, feats(c)], dev(z_, y, x, k)),
+                    cond=cond, width=2, shift=c, batch=("t4", tag), total=lambda: xt.at[pl.ds(0, 2)],
                 )
-        net.send("ts", lambda: (tok.at[rows(o), :], xt.at[z, :, feats(c)], sibling))
+        net.send("ts", lambda: (tokv.at[rows(o), :], xt.at[z, :, feats(c)], sibling), cond=cond)
 
     def relay_tokens():
         for key, who, half, to in (("tm", zm, 0, zp), ("tp", zp, 1, zm)):
@@ -354,10 +392,14 @@
     def dot(lhs, rhs):
         return jnp.dot(lhs, rhs, preferred_element_type=F32)
 
+    staged(0)
     exchange(0)
-    spread_tokens()
+    stage_t.wait()
+    staged(1)
+    exchange(1)
+    spread_tokens(0, taker)
     start(0)
-    exchange(1)
+    start(1)
     exchange(2)
     net.send("ps", lambda: (pool, pw.at[c, o, y, x], sibling), cond=taker)
     net.send("pz", lambda: (pool, pw.at[c, j, y, x], dev(zp, y, x, j)), width=2, shift=c)
@@ -369,15 +411,14 @@
     sa[0].two()
     sb[0].two()
     gain1 = g1[...]
-    own_tok.wait()
-    net.recv("ts", xt.at[z, :, feats(o)])
-    n[pl.ds(0, ROWS), :] = normed(xt[z], gain1)
+    sa[0].pre()
+    sb[0].pre()
+    spread_tokens(1, keeper)
     sa[0].three()
     sb[0].three()
     relay_tokens()
     sa[0].four()
     sb[0].four()
-    start(1)
 
     @pl.when(keeper)
     def _():
@@ -389,9 +430,11 @@
         net.recv("pz", pw.at[0, c, y, x], 0, 2)
         net.recv("pz", pw.at[1, c, y, x], 1, 2)
 
-    spool.one()
-    spool.then()
+    spool.first()
     start(2)
+    own_tok.wait()
+    net.recv("ts", xt.at[z, :, feats(o)])
+    n[pl.ds(0, ROWS), :] = normed(xt[z], gain1)
     n[pl.ds(ROWS, ROWS), :] = normed(xt[zm], gain1)
     n[pl.ds(2 * ROWS, ROWS), :] = normed(xt[zp], gain1)
     net.recv("to", xt.at[zo])
@@ -399,6 +442,9 @@
     sa[0].five()
     sb[0].five()
     turn(0, c, wd1, 0)
+    sa[1].two()
+    sb[1].two()
+    spool.second()
     handed(0)
 
     gate_up(0, 3 * ROWS, ROWS, put1(3 * ROWS, ROWS))
@@ -406,9 +452,8 @@
     so[...] = dot(h1[pl.ds(3 * ROWS, ROWS), :], wd1[...]).astype(BF16)
     net.send("r0", lambda: (so.at[:, feats(0)], ra.at[0], dev(zp, y, x, c)), batch="r", total=lambda: so)
     net.send("r1", lambda: (so.at[:, feats(1)], ra.at[1], dev(zm, y, x, c)), batch="r", total=lambda: so)
-    sa[1].two()
-    sb[1].two()
-    spool.two()
+    sa[2].two()
+    sb[2].two()
     gate_up(0, ROWS, 2 * ROWS, put1(ROWS, 2 * ROWS))
     sums = dot(h1[pl.ds(ROWS, 2 * ROWS), :], wd1[...])
     sm[:, :HALF] = sums[:ROWS, :HALF].astype(BF16)
@@ -425,32 +470,29 @@
 
     pass_on("qm", sp, 0, 1, zp)
     pass_on("qp", sm, 1, 0, zm)
+    sa[1].pre()
+    sb[1].pre()
+    gate_up(0, 0, ROWS, put1(0, ROWS))
+    own1[...] = dot(h1[pl.ds(0, ROWS), :], wd1[...])
     sa[1].three()
     sb[1].three()
-    spool.three()
-    gate_up(0, 0, ROWS, put1(0, ROWS))
-    own1[...] = dot(h1[pl.ds(0, ROWS), :], wd1[...])
     net.recv("r0", ra.at[0])
     sp[:, :HALF] = (pp[...] + ra[0].astype(F32)).astype(BF16)
     net.recv("r1", ra.at[1])
     sm[:, HALF:] = (pm[...] + ra[1].astype(F32)).astype(BF16)
     pass_on("qm", sp, 0, 0, zp)
     pass_on("qp", sm, 1, 1, zm)
-    sa[2].two()
-    sb[2].two()
+    spool.third()
+    sa[2].pre()
+    sb[2].pre()
     sa[1].four()
     sb[1].four()
-    spool.four()
     sa[2].three()
     sb[2].three()
-    spool.five()
-    net.recv(("p", "d"), pw.at[:, o])
+    spool.last(o)
     for g in range(4):
         wide = pw[g // 2].reshape(32, 16, 256).astype(F32)
         maps[g] = wide[:, 8 * (g % 2) : 8 * (g % 2) + 8, :].reshape(256, 256).astype(BF16).T
-    sa[1].five()
-    sb[1].five()
-    turn(1, c, wd2, 0)
     for key, k, half in (("qm", 0, 1), ("qp", 1, 0), ("qm", 0, 0), ("qp", 1, 1)):
         net.recv(f"{key}{half}", rb.at[k, :, feats(half)])
     block = own1[...] + rb[0].astype(F32) + rb[1].astype(F32)
@@ -481,8 +523,11 @@
     net.send("a", lambda: (ob, xq, dev(zq, y, x, c)))
     gain2 = g2[...]
     n[pl.ds(0, ROWS), :] = normed(ob[...], gain2)
+    sa[1].five()
+    sb[1].five()
     sa[2].four()
     sb[2].four()
+    turn(1, c, wd2, 0)
     handed(1)
     gate_up(1, 0, ROWS, put2(0, ROWS, 0))
     turn(1, o, wd2, 0)
@@ -549,6 +594,8 @@
             pltpu.VMEM((2, ROWS, HALF), BF16),
             pltpu.VMEM((ROWS, D), F32),
             pltpu.VMEM((ROWS, HALF), F32),
+            pltpu.VMEM((2, 3, 32, 1280), BF16),
+            pltpu.VMEM((256, HALF), BF16),
             pltpu.SemaphoreType.DMA((N_SEND,)),
             pltpu.SemaphoreType.DMA((N_RECV,)),
             pltpu.SemaphoreType.DMA((N_LOCAL,)),

time: 67.1 us -> 62.7 us (0.934)
  Pallas kernels: 65.2 us -> 60.9 us
    pallas_call x1, Pallas kernels: 65.2 us -> 60.9 us  [local(): pl.pallas_call(kernel, out_shape=jax.ShapeDtypeStruct((256, HALF), BF16),...]
where the time goes in v4:
time: 62.7 us; the launch traced here: 62.6 us
  Pallas kernels  60.9 us (97%)
  local copies, waits for them, and re-layouts  1.67 us (3%)
    pallas_call x1, Pallas kernels, local(): pl.pallas_call(kernel, out_shape=jax.ShapeDtypeStruct((256, HALF), BF16),...  60.9 us
    unnamed x1, local copies, waits for them, and re-layouts  1.67 us

profile of v4, /device:TPU:1, one launch (start us, length us, event | category | flops | bytes accessed | tf_op | source)
XLA Modules:
  0.0 62.6 jit_solution(3839372430001030150)
XLA Ops:
  0.0 60.9 %shard_map.118 = bf16[256,512]{1,0:T(8,128)(2,1)} custom-call(bf16[256,512]{1,0:T(8,128)(2,1)} %bitcast.12, f32[1,1024]{1,0:T(1,128)} %bitcast.16, bf16[32,1280]{1,0:T(8,128)(2,1)} %gate1.1, bf16[32,1280]{1,0:T(8,128)(2,1)} %up1.1, bf16[32,1280]{1,0:T(8,128)(2,1)} %bitcast.13, f32[1,512]{1,0:T(1,128)} %bitcast.18, bf16[16,256]{1,0:T(8,128)(2,1)} %bitcast.15, ...), custom_call_target="tpu_custom_call" | custom-call | tf_op jit(solution)/shard_map/pallas_call | solution.py:564
  60.9 1.7 %copy.14 = bf16[1,256,512]{2,1,0:T(8,128)(2,1)} copy(bf16[1,256,512]{2,1,0:T(8,128)(2,1)} %bitcast.11) | data formatting | bytes 524288

commit v5 on v4

--- a/solution.py
+++ b/solution.py
@@ -14,8 +14,8 @@
 ROWS = 128
 UNIT = 640
 DIRECT = True
-N_SEND = 35
-N_RECV = 90
+N_SEND = 36
+N_RECV = 92
 N_LOCAL = 10
 
 
@@ -123,12 +123,12 @@
         self.both(0, self.a)
 
     def two(self):
+        self.recv("1p", self.ap, self.b)
+        if not self.direct:
+            self.send("1o", self.ap, self.b, self.to_am, "far", 1)
+        self.both(2, self.ap)
         self.recv("1m", self.am, self.b)
-        if not self.direct:
-            self.send("1o", self.am, self.b, self.to_ap, "far", 1)
         self.both(1, self.am)
-        self.recv("1p", self.ap, self.b)
-        self.both(2, self.ap)
 
     def three(self):
         self.recv("1o", self.ao, self.b)
@@ -157,28 +157,42 @@
 
 
 class Coarse:
-    def __init__(self, net, buf, c, y, x, to_row, to_column, sibling):
+    def __init__(self, net, buf, c, y, x, to_row, column, sibling):
         self.net, self.buf, self.c, self.y, self.x = net, buf, c, y, x
-        self.to_row, self.to_column, self.sibling = to_row, to_column, sibling
-
-    def send(self, key, make, device, size):
-        self.net.send(key, lambda: (make(), make(), device), batch=key, total=lambda: size)
+        self.to_row, self.sibling = to_row, sibling
+        _, self.yp, self.ym, self.yo, self.to_yp, self.to_ym, _ = column
+
+    def send(self, key, make, device, batch, total):
+        self.net.send(key, lambda: (make(), make(), device), batch=batch, total=lambda: total)
+
+    def row(self, y):
+        return self.buf.at[:, self.c, y]
+
+    def part(self, y, k):
+        return self.buf.at[:, self.c, y, pl.ds(2 * k, 2)]
 
     def first(self):
         for device in self.to_row:
-            self.send("p1", lambda: self.buf.at[:, self.c, self.y, self.x], device, self.buf.at[:, 0, 0, pl.ds(0, 3)])
+            self.send(
+                "p1", lambda: self.buf.at[:, self.c, self.y, self.x], device, "p1", self.buf.at[:, 0, 0, pl.ds(0, 3)]
+            )
 
     def second(self):
         self.net.recv("p1", self.buf.at[:, 0, 0, pl.ds(0, 3)])
-        for device in self.to_column:
-            self.send("p2", lambda: self.buf.at[:, self.c, self.y], device, self.buf.at[:, 0, pl.ds(0, 3)])
+        for key, device in (("p2m", self.to_yp), ("p2p", self.to_ym)):
+            self.send(key, lambda: self.row(self.y), device, "p2", self.buf.at[:, 0, pl.ds(0, 2)])
 
     def third(self):
-        self.net.recv("p2", self.buf.at[:, 0, pl.ds(0, 3)])
-        self.send("p3", lambda: self.buf.at[:, self.c], self.sibling, self.buf.at[:, 0])
+        for key, y, k, device in (("p2m", self.ym, 0, self.to_yp), ("p2p", self.yp, 1, self.to_ym)):
+            self.net.recv(key, self.row(y))
+            self.send("p3", lambda y=y, k=k: self.part(y, k), device, "p3", self.row(0))
+
+    def fourth(self):
+        self.net.recv("p3", self.row(self.yo))
+        self.send("p4", lambda: self.buf.at[:, self.c], self.sibling, "p4", self.buf.at[:, 0])
 
     def last(self, o):
-        self.net.recv("p3", self.buf.at[:, o])
+        self.net.recv("p4", self.buf.at[:, o])
 
 
 def normed(values, gain):
@@ -326,7 +340,7 @@
 
     sa = [stream_a(u) for u in range(3)]
     sb = [stream_b(u) for u in range(3)]
-    spool = Coarse(net, pw, c, y, x, (in_x[4], in_x[5], in_x[6]), (in_y[4], in_y[5], in_y[6]), sibling)
+    spool = Coarse(net, pw, c, y, x, (in_x[4], in_x[5], in_x[6]), in_y, sibling)
 
     def start(u):
         own(u)
@@ -470,6 +484,7 @@
 
     pass_on("qm", sp, 0, 1, zp)
     pass_on("qp", sm, 1, 0, zm)
+    spool.third()
     sa[1].pre()
     sb[1].pre()
     gate_up(0, 0, ROWS, put1(0, ROWS))
@@ -482,13 +497,13 @@
     sm[:, HALF:] = (pm[...] + ra[1].astype(F32)).astype(BF16)
     pass_on("qm", sp, 0, 0, zp)
     pass_on("qp", sm, 1, 1, zm)
-    spool.third()
+    sa[2].three()
+    sb[2].three()
     sa[2].pre()
     sb[2].pre()
+    spool.fourth()
     sa[1].four()
     sb[1].four()
-    sa[2].three()
-    sb[2].three()
     spool.last(o)
     for g in range(4):
         wide = pw[g // 2].reshape(32, 16, 256).astype(F32)
@@ -563,7 +578,7 @@
     vmem = pl.BlockSpec(memory_space=pltpu.VMEM)
     result = pl.pallas_call(
         kernel,
-        out_shape=jax.ShapeDtypeStruct((256, HALF), BF16),
+        out_shape=pltpu.VMEM((256, HALF), BF16),
         in_specs=[hbm, vmem, hbm, hbm, hbm, hbm, hbm, hbm, vmem, hbm, hbm, hbm],
         out_specs=vmem,
         scratch_shapes=[
@@ -600,10 +615,15 @@
             pltpu.SemaphoreType.DMA((N_RECV,)),
             pltpu.SemaphoreType.DMA((N_LOCAL,)),
         ],
-        compiler_params=pltpu.CompilerParams(collective_id=0, has_side_effects=True, vmem_limit_bytes=67043328),
+        compiler_params=pltpu.CompilerParams(collective_id=0, has_side_effects=True, vmem_limit_bytes=52 * 2**20),
     )(
-        tok.reshape(256, HALF), g1.reshape(1, D), gate1, up1, down1.T, mixg.reshape(1, HALF),
-        pool.transpose(0, 2, 1).reshape(16, 256), scale.reshape(1, HALF), g2.reshape(1, D), gate2, up2, down2.T,
+        *(
+            pltpu.with_memory_space_constraint(value, pltpu.HBM)
+            for value in (
+                tok.reshape(256, HALF), g1.reshape(1, D), gate1, up1, down1.T, mixg.reshape(1, HALF),
+                pool.transpose(0, 2, 1).reshape(16, 256), scale.reshape(1, HALF), g2.reshape(1, D), gate2, up2, down2.T,
+            )
+        )
     )
     return result.reshape(1, 256, HALF)
 

time: 62.7 us -> 59.7 us (0.952)
  Pallas kernels: 60.9 us -> 58.8 us
  local copies, waits for them, and re-layouts: 1.67 us -> 0.71 us
    pallas_call x1, Pallas kernels: 60.9 us -> 58.8 us  [local(): pl.pallas_call(kernel, out_shape=pltpu.VMEM((256, HALF), BF16), in_specs=...]
    unnamed x1, local copies, waits for them, and re-layouts: 1.67 us -> 0.71 us
where the time goes in v5:
time: 59.7 us; the launch traced here: 59.5 us
  Pallas kernels  58.8 us (98%)
  local copies, waits for them, and re-layouts  0.71 us (1%)
    pallas_call x1, Pallas kernels, local(): pl.pallas_call(kernel, out_shape=pltpu.VMEM((256, HALF), BF16), in_specs=...  58.8 us

profile of v5, /device:TPU:1, one launch (start us, length us, event | category | flops | bytes accessed | tf_op | source)
XLA Modules:
  0.0 59.5 jit_solution(15266014670564884489)
XLA Ops:
  0.0 58.8 %shard_map.118 = bf16[256,512]{1,0:T(8,128)(2,1)S(1)} custom-call(bf16[256,512]{1,0:T(8,128)(2,1)} %bitcast.12, f32[1,1024]{1,0:T(1,128)} %bitcast.16, bf16[32,1280]{1,0:T(8,128)(2,1)} %gate1.1, bf16[32,1280]{1,0:T(8,128)(2,1)} %up1.1, bf16[32,1280]{1,0:T(8,128)(2,1)} %bitcast.13, f32[1,512]{1,0:T(1,128)} %bitcast.18, bf16[16,256]{1,0:T(8,128)(2,1)} %bitcast.15, ...), custom_call_target="tpu_custom_call" | custom-call | tf_op jit(solution)/shard_map/pallas_call | solution.py:579
  58.8 0.7 %copy.14 = bf16[1,256,512]{2,1,0:T(8,128)(2,1)} copy(bf16[1,256,512]{2,1,0:T(8,128)(2,1)S(1)} %bitcast.11) | data formatting | bytes 524288

commit v6 on v5

--- a/solution.py
+++ b/solution.py
@@ -88,6 +88,7 @@
         self.a, self.ap, self.am, self.ao, self.to_ap, self.to_am, self.to_ao = first
         self.b, self.bp, self.bm, self.bo, self.to_bp, self.to_bm, self.to_bo = second
         self.sibling = sibling
+        self.flip = unit == 2
 
     def send(self, what, a, b, device, kind, count):
         self.net.send(
@@ -123,12 +124,11 @@
         self.both(0, self.a)
 
     def two(self):
-        self.recv("1p", self.ap, self.b)
-        if not self.direct:
-            self.send("1o", self.ap, self.b, self.to_am, "far", 1)
-        self.both(2, self.ap)
-        self.recv("1m", self.am, self.b)
-        self.both(1, self.am)
+        for key, k, a, to in (("1p", 2, self.ap, self.to_am), ("1m", 1, self.am, self.to_ap))[:: -1 if self.flip else 1]:
+            self.recv(key, a, self.b)
+            if key == ("1m" if self.flip else "1p") and not self.direct:
+                self.send("1o", a, self.b, to, "far", 1)
+            self.both(k, a)
 
     def three(self):
         self.recv("1o", self.ao, self.b)
@@ -203,7 +203,7 @@
 
 def kernel(
     tok, g1, gate1, up1, down1, mixg, pool, scale, g2, gate2, up2, down2, out,
-    w, pw, xt, xq, n, h1, h2, wd1, wd2, maps, own1, pm, pp, so, sm, sp, ra, rb, a1, hs, hr, mg, ob, sq, rq, base, rx, st, tokv,
+    w, pw, xt, xq, n, h1, h2, wd1, wd2, maps, own1, pm, pp, so, sm, sp, ra, rb, a1, hs, hr, mg, ob, sq, rq, base, rx, st, tokv, gu, part1,
     ss, rs, ls,
 ):
     rep = lax.axis_index("rep")
@@ -375,6 +375,9 @@
         net.recv("tm", xt.at[zm, :, feats(1)], 1, 2)
         net.recv("tp", xt.at[zp, :, feats(0)], 0, 2)
 
+    def dot(lhs, rhs):
+        return jnp.dot(lhs, rhs, preferred_element_type=F32)
+
     def gate_up(u, at, count, put):
         for k in range(UNIT // 128):
             part = pl.ds(k * 128, 128)
@@ -398,13 +401,181 @@
 
         return put
 
+    def gate_up_half(u, at, count, part, put=None):
+        lanes = feats(part)
+        for k in range(UNIT // 128):
+            hid = pl.ds(k * 128, 128)
+            wg = w[u, 0, part, :, :, :, hid].reshape(HALF, 128)
+            wu = w[u, 1, part, :, :, :, hid].reshape(HALF, 128)
+            both = dot(n[pl.ds(at, count), lanes], jnp.concatenate([wg, wu], axis=1))
+            if put is None:
+                gu[:, pl.ds(k * 256, 256)] = both
+            else:
+                both = both + gu[:, pl.ds(k * 256, 256)]
+                gate, up = both[:, :128], both[:, 128:]
+                put(k * 128, (gate * jax.nn.sigmoid(gate) * up).astype(BF16))
+
     def turn(u, part, wide, at):
         for k in range(2):
             block = w[u, 2, part, 2 * k : 2 * k + 2].reshape(256, UNIT)
             wide[pl.ds(at, UNIT), pl.ds(pl.multiple_of(part * HALF + 256 * k, 128), 256)] = block.T
 
-    def dot(lhs, rhs):
-        return jnp.dot(lhs, rhs, preferred_element_type=F32)
+    def start_pool():
+        @pl.when(keeper)
+        def _():
+            own_pool().wait()
+            net.recv("ps", pw.at[o, c, y, x])
+
+        @pl.when(taker)
+        def _():
+            net.recv("pz", pw.at[0, c, y, x], 0, 2)
+            net.recv("pz", pw.at[1, c, y, x], 1, 2)
+
+        spool.first()
+
+    def norm_own():
+        own_tok.wait()
+        net.recv("ts", xt.at[z, :, feats(o)])
+        n[pl.ds(0, ROWS), :] = normed(xt[z], gain1)
+
+    def norm_next():
+        n[pl.ds(ROWS, ROWS), :] = normed(xt[zm], gain1)
+        n[pl.ds(2 * ROWS, ROWS), :] = normed(xt[zp], gain1)
+
+    def norm_last():
+        net.recv("to", xt.at[zo])
+        n[pl.ds(3 * ROWS, ROWS), :] = normed(xt[zo], gain1)
+
+    def first_near():
+        turn(0, c, wd1, 0)
+        gate_up_half(0, 3 * ROWS, ROWS, c)
+
+    def first_opposite():
+        gate_up_half(0, 3 * ROWS, ROWS, o, put1(3 * ROWS, ROWS))
+        turn(0, o, wd1, 0)
+        for k, z_ in ((0, zp), (1, zm)):
+            lanes = slice(HALF * k, HALF * k + HALF)
+            so[:, lanes] = dot(h1[pl.ds(3 * ROWS, ROWS), :], wd1[:, lanes]).astype(BF16)
+            net.send(
+                f"r{k}", lambda k=k, z_=z_: (so.at[:, feats(k)], ra.at[k], dev(z_, y, x, c)), batch="r", total=lambda: so
+            )
+
+    def pass_on(key, buf, k, half, z_):
+        net.send(
+            f"{key}{half}",
+            lambda: (buf.at[:, feats(half)], rb.at[k, :, feats(half)], dev(z_, y, x, c)),
+            batch="q", total=lambda: xt.at[two],
+        )
+
+    def first_neighbours():
+        gate_up(0, ROWS, 2 * ROWS, put1(ROWS, 2 * ROWS))
+        sums = dot(h1[pl.ds(ROWS, 2 * ROWS), :], wd1[...])
+        sm[:, :HALF] = sums[:ROWS, :HALF].astype(BF16)
+        sp[:, HALF:] = sums[ROWS:, HALF:].astype(BF16)
+        pm[...] = sums[:ROWS, HALF:]
+        pp[...] = sums[ROWS:, :HALF]
+        pass_on("qm", sp, 0, 1, zp)
+        pass_on("qp", sm, 1, 0, zm)
+
+    def first_own():
+        gate_up(0, 0, ROWS, put1(0, ROWS))
+        own1[...] = dot(h1[pl.ds(0, ROWS), :], wd1[...])
+
+    def first_pass_on():
+        net.recv("r0", ra.at[0])
+        sp[:, :HALF] = (pp[...] + ra[0].astype(F32)).astype(BF16)
+        pass_on("qm", sp, 0, 0, zp)
+        net.recv("r1", ra.at[1])
+        sm[:, HALF:] = (pm[...] + ra[1].astype(F32)).astype(BF16)
+        pass_on("qp", sm, 1, 1, zm)
+
+    def pool_maps():
+        spool.last(o)
+        for g in range(4):
+            wide = pw[g // 2].reshape(32, 16, 256).astype(F32)
+            maps[g] = wide[:, 8 * (g % 2) : 8 * (g % 2) + 8, :].reshape(256, 256).astype(BF16).T
+
+    def joined(k):
+        return jnp.concatenate([mg[k, 0], mg[k, 1]], axis=1)
+
+    def first_sum():
+        for key, k, half in (("qm", 0, 1), ("qp", 1, 0), ("qm", 0, 0), ("qp", 1, 1)):
+            net.recv(f"{key}{half}", rb.at[k, :, feats(half)])
+        net.recv("mg", mg.at[:, o])
+
+    def halo():
+        for part in (slice(ROWS - 16, ROWS), slice(0, ROWS - 16)):
+            block = own1[part] + rb[0, part].astype(F32) + rb[1, part].astype(F32)
+            value = (xt[z, part].astype(F32) + 0.5 * block).astype(BF16)
+            a1[part] = value
+            hs[part] = normed(value, joined(0))
+            if part.start:
+                net.send("h", lambda: (hs.at[pl.ds(112, 16), :], hr, sibling))
+
+    def mix():
+        net.recv("h", hr)
+        before = jnp.where(c == 1, hr[...].astype(F32), 0.0)
+        floats = hs[...].astype(F32)
+        longer = jnp.concatenate([before, floats], axis=0)
+        positions = c * ROWS + lax.broadcasted_iota(jnp.int32, (ROWS, 256), 0)
+        mix_scale = joined(1)
+        for g in range(4):
+            lanes = slice(256 * g, 256 * g + 256)
+            total = longer[:, lanes]
+            for k in range(g + 1):
+                total = total + pltpu.roll(total, 2**k, axis=0)
+            counts = jnp.minimum(positions + 1, 2 ** (g + 1)).astype(F32)
+            diff = (total[16:] / counts - floats[:, lanes]).astype(BF16)
+            mixed = dot(diff, maps[g])
+            after = a1[:, lanes].astype(F32) + mixed * mix_scale[:, lanes]
+            ob[:, lanes] = after.astype(BF16)
+            if g % 2:
+                half = feats(g // 2)
+                net.send(
+                    "a", lambda half=half: (ob.at[:, half], xq.at[:, half], dev(zq, y, x, c)), batch="a", total=lambda: ob
+                )
+
+    def second_norm():
+        n[pl.ds(0, ROWS), :] = normed(ob[...], gain2)
+
+    def second_own_1():
+        turn(1, 0, wd2, 0)
+        turn(1, 1, wd2, 0)
+        gate_up(1, 0, ROWS, put2(0, ROWS, 0))
+
+    def second_peer_1():
+        net.recv("a", xq)
+        n[pl.ds(ROWS, ROWS), :] = normed(xq[...], gain2)
+        gate_up(1, ROWS, ROWS, put2(ROWS, ROWS, 0))
+        part1[...] = dot(h2[pl.ds(ROWS, ROWS), :UNIT], wd2[:UNIT])
+
+    def second_near():
+        turn(2, c, wd2, UNIT)
+        gate_up_half(2, ROWS, ROWS, c)
+
+    def second_peer_2():
+        gate_up_half(2, ROWS, ROWS, o, put2(ROWS, ROWS, UNIT))
+        turn(2, o, wd2, UNIT)
+        for k in range(2):
+            lanes = slice(HALF * k, HALF * k + HALF)
+            sq[:, lanes] = (part1[:, lanes] + dot(h2[pl.ds(ROWS, ROWS), UNIT:], wd2[UNIT:, lanes])).astype(BF16)
+            net.send(
+                "b",
+                lambda k=k: (sq.at[:, feats(k)], rq.at[c], dev(zq, y, x, k)),
+                width=2, shift=c, batch="b", total=lambda: sq,
+            )
+
+    def second_own_2():
+        gate_up(2, 0, ROWS, put2(0, ROWS, UNIT))
+        base[...] = ob[...].astype(F32) + 0.5 * dot(h2[pl.ds(0, ROWS), :], wd2[...])
+        net.send("f", lambda: (base.at[:, feats(o)], rx, sibling))
+
+    def last_sum():
+        net.recv("f", rx)
+        net.recv("b", rq.at[c], c, 2)
+        out[rows(c), :] = (base[:, feats(c)] + 0.5 * rq[c].astype(F32)).astype(BF16)
+        net.recv("b", rq.at[o], o, 2)
+        out[rows(o), :] = (rx[...] + 0.5 * rq[o].astype(F32)).astype(BF16)
 
     staged(0)
     exchange(0)
@@ -421,10 +592,10 @@
     own_sc.wait()
     net.send("mg", lambda: (mixg, mg.at[0, c], sibling), batch="mg", total=lambda: mg.at[:, 0])
     net.send("mg", lambda: (scale, mg.at[1, c], sibling), batch="mg", total=lambda: mg.at[:, 0])
-
+    gain1 = g1[...]
+    gain2 = g2[...]
     sa[0].two()
     sb[0].two()
-    gain1 = g1[...]
     sa[0].pre()
     sb[0].pre()
     spread_tokens(1, keeper)
@@ -433,70 +604,29 @@
     relay_tokens()
     sa[0].four()
     sb[0].four()
-
-    @pl.when(keeper)
-    def _():
-        own_pool().wait()
-        net.recv("ps", pw.at[o, c, y, x])
-
-    @pl.when(taker)
-    def _():
-        net.recv("pz", pw.at[0, c, y, x], 0, 2)
-        net.recv("pz", pw.at[1, c, y, x], 1, 2)
-
-    spool.first()
+    start_pool()
     start(2)
-    own_tok.wait()
-    net.recv("ts", xt.at[z, :, feats(o)])
-    n[pl.ds(0, ROWS), :] = normed(xt[z], gain1)
-    n[pl.ds(ROWS, ROWS), :] = normed(xt[zm], gain1)
-    n[pl.ds(2 * ROWS, ROWS), :] = normed(xt[zp], gain1)
-    net.recv("to", xt.at[zo])
-    n[pl.ds(3 * ROWS, ROWS), :] = normed(xt[zo], gain1)
+    norm_own()
+    norm_next()
+    norm_last()
     sa[0].five()
     sb[0].five()
-    turn(0, c, wd1, 0)
+    first_near()
     sa[1].two()
     sb[1].two()
     spool.second()
     handed(0)
-
-    gate_up(0, 3 * ROWS, ROWS, put1(3 * ROWS, ROWS))
-    turn(0, o, wd1, 0)
-    so[...] = dot(h1[pl.ds(3 * ROWS, ROWS), :], wd1[...]).astype(BF16)
-    net.send("r0", lambda: (so.at[:, feats(0)], ra.at[0], dev(zp, y, x, c)), batch="r", total=lambda: so)
-    net.send("r1", lambda: (so.at[:, feats(1)], ra.at[1], dev(zm, y, x, c)), batch="r", total=lambda: so)
+    first_opposite()
     sa[2].two()
     sb[2].two()
-    gate_up(0, ROWS, 2 * ROWS, put1(ROWS, 2 * ROWS))
-    sums = dot(h1[pl.ds(ROWS, 2 * ROWS), :], wd1[...])
-    sm[:, :HALF] = sums[:ROWS, :HALF].astype(BF16)
-    sp[:, HALF:] = sums[ROWS:, HALF:].astype(BF16)
-    pm[...] = sums[:ROWS, HALF:]
-    pp[...] = sums[ROWS:, :HALF]
-
-    def pass_on(key, buf, k, half, z_):
-        net.send(
-            f"{key}{half}",
-            lambda: (buf.at[:, feats(half)], rb.at[k, :, feats(half)], dev(z_, y, x, c)),
-            batch="q", total=lambda: xt.at[two],
-        )
-
-    pass_on("qm", sp, 0, 1, zp)
-    pass_on("qp", sm, 1, 0, zm)
+    first_neighbours()
     spool.third()
     sa[1].pre()
     sb[1].pre()
-    gate_up(0, 0, ROWS, put1(0, ROWS))
-    own1[...] = dot(h1[pl.ds(0, ROWS), :], wd1[...])
+    first_own()
     sa[1].three()
     sb[1].three()
-    net.recv("r0", ra.at[0])
-    sp[:, :HALF] = (pp[...] + ra[0].astype(F32)).astype(BF16)
-    net.recv("r1", ra.at[1])
-    sm[:, HALF:] = (pm[...] + ra[1].astype(F32)).astype(BF16)
-    pass_on("qm", sp, 0, 0, zp)
-    pass_on("qp", sm, 1, 1, zm)
+    first_pass_on()
     sa[2].three()
     sb[2].three()
     sa[2].pre()
@@ -504,72 +634,25 @@
     spool.fourth()
     sa[1].four()
     sb[1].four()
-    spool.last(o)
-    for g in range(4):
-        wide = pw[g // 2].reshape(32, 16, 256).astype(F32)
-        maps[g] = wide[:, 8 * (g % 2) : 8 * (g % 2) + 8, :].reshape(256, 256).astype(BF16).T
-    for key, k, half in (("qm", 0, 1), ("qp", 1, 0), ("qm", 0, 0), ("qp", 1, 1)):
-        net.recv(f"{key}{half}", rb.at[k, :, feats(half)])
-    block = own1[...] + rb[0].astype(F32) + rb[1].astype(F32)
-    a1[...] = (xt[z].astype(F32) + 0.5 * block).astype(BF16)
-
-    net.recv("mg", mg.at[:, o])
-    mix_gain = jnp.concatenate([mg[0, 0], mg[0, 1]], axis=1)
-    mix_scale = jnp.concatenate([mg[1, 0], mg[1, 1]], axis=1)
-    hidden = normed(a1[...], mix_gain)
-    hs[...] = hidden
-    net.send("h", lambda: (hs.at[pl.ds(112, 16), :], hr, sibling))
-    net.recv("h", hr)
-    before = jnp.where(c == 1, hr[...].astype(F32), 0.0)
-    floats = hs[...].astype(F32)
-    longer = jnp.concatenate([before, floats], axis=0)
-    positions = c * ROWS + lax.broadcasted_iota(jnp.int32, (ROWS, 256), 0)
-    for g in range(4):
-        lanes = slice(256 * g, 256 * g + 256)
-        total = longer[:, lanes]
-        for k in range(g + 1):
-            total = total + pltpu.roll(total, 2**k, axis=0)
-        counts = jnp.minimum(positions + 1, 2 ** (g + 1)).astype(F32)
-        diff = (total[16:] / counts - floats[:, lanes]).astype(BF16)
-        mixed = dot(diff, maps[g])
-        after = a1[:, lanes].astype(F32) + mixed * mix_scale[:, lanes]
-        ob[:, lanes] = after.astype(BF16)
-
-    net.send("a", lambda: (ob, xq, dev(zq, y, x, c)))
-    gain2 = g2[...]
-    n[pl.ds(0, ROWS), :] = normed(ob[...], gain2)
+    pool_maps()
+    first_sum()
+    halo()
+    mix()
     sa[1].five()
     sb[1].five()
     sa[2].four()
     sb[2].four()
-    turn(1, c, wd2, 0)
+    second_norm()
     handed(1)
-    gate_up(1, 0, ROWS, put2(0, ROWS, 0))
-    turn(1, o, wd2, 0)
+    second_own_1()
     sa[2].five()
     sb[2].five()
-    turn(2, c, wd2, UNIT)
-    net.recv("a", xq)
-    n[pl.ds(ROWS, ROWS), :] = normed(xq[...], gain2)
-    gate_up(1, ROWS, ROWS, put2(ROWS, ROWS, 0))
+    second_peer_1()
+    second_near()
     handed(2)
-    gate_up(2, ROWS, ROWS, put2(ROWS, ROWS, UNIT))
-    turn(2, o, wd2, UNIT)
-    sq[...] = dot(h2[pl.ds(ROWS, ROWS), :], wd2[...]).astype(BF16)
-    for k in range(2):
-        net.send(
-            "b",
-            lambda k=k: (sq.at[:, feats(k)], rq.at[c], dev(zq, y, x, k)),
-            width=2, shift=c, batch="b", total=lambda: sq,
-        )
-    gate_up(2, 0, ROWS, put2(0, ROWS, UNIT))
-    base[...] = ob[...].astype(F32) + 0.5 * dot(h2[pl.ds(0, ROWS), :], wd2[...])
-    net.send("f", lambda: (base.at[:, feats(o)], rx, sibling))
-    net.recv("b", rq.at[c], c, 2)
-    out[rows(c), :] = (base[:, feats(c)] + 0.5 * rq[c].astype(F32)).astype(BF16)
-    net.recv("f", rx)
-    net.recv("b", rq.at[o], o, 2)
-    out[rows(o), :] = (rx[...] + 0.5 * rq[o].astype(F32)).astype(BF16)
+    second_peer_2()
+    second_own_2()
+    last_sum()
     net.finish()
 
 
@@ -611,6 +694,8 @@
             pltpu.VMEM((ROWS, HALF), F32),
             pltpu.VMEM((2, 3, 32, 1280), BF16),
             pltpu.VMEM((256, HALF), BF16),
+            pltpu.VMEM((ROWS, 2 * UNIT), F32),
+            pltpu.VMEM((ROWS, D), F32),
             pltpu.SemaphoreType.DMA((N_SEND,)),
             pltpu.SemaphoreType.DMA((N_RECV,)),
             pltpu.SemaphoreType.DMA((N_LOCAL,)),

time: 59.7 us -> 58.9 us (0.987)
  Pallas kernels: 58.8 us -> 58 us
    pallas_call x1, Pallas kernels: 58.8 us -> 58 us  [local(): pl.pallas_call(kernel, out_shape=pltpu.VMEM((256, HALF), BF16), in_specs=...]
where the time goes in v6:
time: 58.9 us; the launch traced here: 58.7 us
  Pallas kernels  58 us (98%)
  local copies, waits for them, and re-layouts  0.71 us (1%)
    pallas_call x1, Pallas kernels, local(): pl.pallas_call(kernel, out_shape=pltpu.VMEM((256, HALF), BF16), in_specs=...  58 us

profile of v6, /device:TPU:1, one launch (start us, length us, event | category | flops | bytes accessed | tf_op | source)
XLA Modules:
  0.0 58.7 jit_solution(10923972544752805541)
XLA Ops:
  0.0 58.0 %shard_map.118 = bf16[256,512]{1,0:T(8,128)(2,1)S(1)} custom-call(bf16[256,512]{1,0:T(8,128)(2,1)} %bitcast.12, f32[1,1024]{1,0:T(1,128)} %bitcast.16, bf16[32,1280]{1,0:T(8,128)(2,1)} %gate1.1, bf16[32,1280]{1,0:T(8,128)(2,1)} %up1.1, bf16[32,1280]{1,0:T(8,128)(2,1)} %bitcast.13, f32[1,512]{1,0:T(1,128)} %bitcast.18, bf16[16,256]{1,0:T(8,128)(2,1)} %bitcast.15, ...), custom_call_target="tpu_custom_call" | custom-call | tf_op jit(solution)/shard_map/pallas_call | solution.py:662
  58.0 0.7 %copy.14 = bf16[1,256,512]{2,1,0:T(8,128)(2,1)} copy(bf16[1,256,512]{2,1,0:T(8,128)(2,1)S(1)} %bitcast.11) | data formatting | bytes 524288

commit v7 on v6

--- a/solution.py
+++ b/solution.py
@@ -14,8 +14,8 @@
 ROWS = 128
 UNIT = 640
 DIRECT = True
-N_SEND = 36
-N_RECV = 92
+N_SEND = 35
+N_RECV = 90
 N_LOCAL = 10
 
 
@@ -139,11 +139,13 @@
         self.recv("2m0", self.a, self.bm)
         self.send("2o", self.a, self.bm, self.to_bp, "on", 4)
 
-    def four(self):
+    def mid(self):
         self.recv("2m1", self.am, self.bm)
         self.send("2o", self.am, self.bm, self.to_bp, "on", 4)
         self.recv("2p2", self.ap, self.bp)
         self.send("2o", self.ap, self.bp, self.to_bm, "on", 4)
+
+    def four(self):
         self.recv("2p3", self.ao, self.bp)
         self.send("2o", self.ao, self.bp, self.to_bm, "on", 4)
         self.net.recv((self.tag, "2p01"), self.size(2))
@@ -157,42 +159,32 @@
 
 
 class Coarse:
-    def __init__(self, net, buf, c, y, x, to_row, column, sibling):
-        self.net, self.buf, self.c, self.y, self.x = net, buf, c, y, x
-        self.to_row, self.sibling = to_row, sibling
-        _, self.yp, self.ym, self.yo, self.to_yp, self.to_ym, _ = column
-
-    def send(self, key, make, device, batch, total):
-        self.net.send(key, lambda: (make(), make(), device), batch=batch, total=lambda: total)
-
-    def row(self, y):
-        return self.buf.at[:, self.c, y]
-
-    def part(self, y, k):
-        return self.buf.at[:, self.c, y, pl.ds(2 * k, 2)]
+    def __init__(self, net, piece, some, first, second, sibling):
+        self.net, self.piece, self.some, self.first_axis, self.second_axis = net, piece, some, first, second
+        self.sibling = sibling
+
+    def send(self, key, a, device, total):
+        self.net.send(
+            key, lambda: (self.piece(a, self.second_axis[0]), self.piece(a, self.second_axis[0]), device),
+            batch=key, total=lambda: total,
+        )
 
     def first(self):
-        for device in self.to_row:
-            self.send(
-                "p1", lambda: self.buf.at[:, self.c, self.y, self.x], device, "p1", self.buf.at[:, 0, 0, pl.ds(0, 3)]
-            )
+        for device in self.first_axis[4:]:
+            self.send("p1", self.first_axis[0], device, self.some(1, 3))
 
     def second(self):
-        self.net.recv("p1", self.buf.at[:, 0, 0, pl.ds(0, 3)])
-        for key, device in (("p2m", self.to_yp), ("p2p", self.to_ym)):
-            self.send(key, lambda: self.row(self.y), device, "p2", self.buf.at[:, 0, pl.ds(0, 2)])
-
-    def third(self):
-        for key, y, k, device in (("p2m", self.ym, 0, self.to_yp), ("p2p", self.yp, 1, self.to_ym)):
-            self.net.recv(key, self.row(y))
-            self.send("p3", lambda y=y, k=k: self.part(y, k), device, "p3", self.row(0))
-
-    def fourth(self):
-        self.net.recv("p3", self.row(self.yo))
-        self.send("p4", lambda: self.buf.at[:, self.c], self.sibling, "p4", self.buf.at[:, 0])
-
-    def last(self, o):
-        self.net.recv("p4", self.buf.at[:, o])
+        self.net.recv("p1", self.some(1, 3))
+        for device in self.second_axis[4:]:
+            for a in self.first_axis[:4]:
+                self.send("p2", a, device, self.some(3, 4))
+
+    def third(self, mine):
+        self.net.recv("p2", self.some(3, 4))
+        self.net.send("p3", lambda: (mine, mine, self.sibling))
+
+    def last(self, theirs):
+        self.net.recv("p3", theirs)
 
 
 def normed(values, gain):
@@ -340,7 +332,18 @@
 
     sa = [stream_a(u) for u in range(3)]
     sb = [stream_b(u) for u in range(3)]
-    spool = Coarse(net, pw, c, y, x, (in_x[4], in_x[5], in_x[6]), in_y, sibling)
+    def pick(k, l):
+        return k * o + l * c
+
+    xs, ys = (x, xp, xm, xo), (y, yp, ym, yo)
+    first = [pick(k, l) for k, l in zip(xs, ys)]
+    second = [pick(l, k) for k, l in zip(xs, ys)]
+    first += [dev(z, pick(y, l), pick(k, x), c) for k, l in zip(xs[1:], ys[1:])]
+    second += [dev(z, pick(l, y), pick(x, k), c) for k, l in zip(xs[1:], ys[1:])]
+    spool = Coarse(
+        net, lambda a, b: pw.at[:, c, pick(b, a), pick(a, b)], lambda k, l: pw.at[:, 0, pl.ds(0, k), pl.ds(0, l)],
+        first, second, sibling,
+    )
 
     def start(u):
         own(u)
@@ -490,7 +493,7 @@
         pass_on("qp", sm, 1, 1, zm)
 
     def pool_maps():
-        spool.last(o)
+        spool.last(pw.at[:, o])
         for g in range(4):
             wide = pw[g // 2].reshape(32, 16, 256).astype(F32)
             maps[g] = wide[:, 8 * (g % 2) : 8 * (g % 2) + 8, :].reshape(256, 256).astype(BF16).T
@@ -602,6 +605,8 @@
     sa[0].three()
     sb[0].three()
     relay_tokens()
+    sa[0].mid()
+    sb[0].mid()
     sa[0].four()
     sb[0].four()
     start_pool()
@@ -620,20 +625,23 @@
     sa[2].two()
     sb[2].two()
     first_neighbours()
-    spool.third()
     sa[1].pre()
     sb[1].pre()
     first_own()
     sa[1].three()
     sb[1].three()
+    sa[1].mid()
+    sb[1].mid()
     first_pass_on()
     sa[2].three()
     sb[2].three()
     sa[2].pre()
     sb[2].pre()
-    spool.fourth()
+    spool.third(pw.at[:, c])
     sa[1].four()
     sb[1].four()
+    sa[2].mid()
+    sb[2].mid()
     pool_maps()
     first_sum()
     halo()

time: 58.9 us -> 57 us (0.968)
  Pallas kernels: 58 us -> 56.1 us
    pallas_call x1, Pallas kernels: 58 us -> 56.1 us  [local(): pl.pallas_call(kernel, out_shape=pltpu.VMEM((256, HALF), BF16), in_specs=...]
where the time goes in v7:
time: 57 us; the launch traced here: 56.8 us
  Pallas kernels  56.1 us (98%)
  local copies, waits for them, and re-layouts  0.71 us (1%)
    pallas_call x1, Pallas kernels, local(): pl.pallas_call(kernel, out_shape=pltpu.VMEM((256, HALF), BF16), in_specs=...  56.1 us

profile of v7, /device:TPU:1, one launch (start us, length us, event | category | flops | bytes accessed | tf_op | source)
XLA Modules:
  0.0 56.8 jit_solution(3306621441010404235)
XLA Ops:
  0.0 56.1 %shard_map.118 = bf16[256,512]{1,0:T(8,128)(2,1)S(1)} custom-call(bf16[256,512]{1,0:T(8,128)(2,1)} %bitcast.12, f32[1,1024]{1,0:T(1,128)} %bitcast.16, bf16[32,1280]{1,0:T(8,128)(2,1)} %gate1.1, bf16[32,1280]{1,0:T(8,128)(2,1)} %up1.1, bf16[32,1280]{1,0:T(8,128)(2,1)} %bitcast.13, f32[1,512]{1,0:T(1,128)} %bitcast.18, bf16[16,256]{1,0:T(8,128)(2,1)} %bitcast.15, ...), custom_call_target="tpu_custom_call" | custom-call | tf_op jit(solution)/shard_map/pallas_call | solution.py:670
  56.1 0.7 %copy.14 = bf16[1,256,512]{2,1,0:T(8,128)(2,1)} copy(bf16[1,256,512]{2,1,0:T(8,128)(2,1)S(1)} %bitcast.11) | data formatting | bytes 524288

commit v8 on v7

--- a/solution.py
+++ b/solution.py
@@ -13,7 +13,7 @@
 HALF = 512
 ROWS = 128
 UNIT = 640
-DIRECT = True
+DIRECT = False
 N_SEND = 35
 N_RECV = 90
 N_LOCAL = 10
@@ -516,27 +516,30 @@
                 net.send("h", lambda: (hs.at[pl.ds(112, 16), :], hr, sibling))
 
     def mix():
-        net.recv("h", hr)
-        before = jnp.where(c == 1, hr[...].astype(F32), 0.0)
-        floats = hs[...].astype(F32)
-        longer = jnp.concatenate([before, floats], axis=0)
-        positions = c * ROWS + lax.broadcasted_iota(jnp.int32, (ROWS, 256), 0)
         mix_scale = joined(1)
-        for g in range(4):
-            lanes = slice(256 * g, 256 * g + 256)
-            total = longer[:, lanes]
-            for k in range(g + 1):
-                total = total + pltpu.roll(total, 2**k, axis=0)
-            counts = jnp.minimum(positions + 1, 2 ** (g + 1)).astype(F32)
-            diff = (total[16:] / counts - floats[:, lanes]).astype(BF16)
-            mixed = dot(diff, maps[g])
-            after = a1[:, lanes].astype(F32) + mixed * mix_scale[:, lanes]
-            ob[:, lanes] = after.astype(BF16)
-            if g % 2:
-                half = feats(g // 2)
-                net.send(
-                    "a", lambda half=half: (ob.at[:, half], xq.at[:, half], dev(zq, y, x, c)), batch="a", total=lambda: ob
-                )
+        for start in (64, 0):
+            part = slice(start, start + 64)
+            if start:
+                longer = hs[48:ROWS].astype(F32)
+            else:
+                net.recv("h", hr)
+                before = jnp.where(c == 1, hr[...].astype(F32), 0.0)
+                longer = jnp.concatenate([before, hs[:64].astype(F32)], axis=0)
+            positions = c * ROWS + start + lax.broadcasted_iota(jnp.int32, (64, 256), 0)
+            for g in range(4):
+                lanes = slice(256 * g, 256 * g + 256)
+                total = longer[:, lanes]
+                for k in range(g + 1):
+                    total = total + pltpu.roll(total, 2**k, axis=0)
+                counts = jnp.minimum(positions + 1, 2 ** (g + 1)).astype(F32)
+                diff = (total[16:] / counts - longer[16:, lanes]).astype(BF16)
+                mixed = dot(diff, maps[g])
+                after = a1[part, lanes].astype(F32) + mixed * mix_scale[:, lanes]
+                ob[part, lanes] = after.astype(BF16)
+            half = pl.ds(start, 64)
+            net.send(
+                "a", lambda half=half: (ob.at[half], xq.at[half], dev(zq, y, x, c)), batch="a", total=lambda: ob
+            )
 
     def second_norm():
         n[pl.ds(0, ROWS), :] = normed(ob[...], gain2)

time: 57 us -> 56.2 us (0.986)
  Pallas kernels: 56.1 us -> 55.3 us
    pallas_call x1, Pallas kernels: 56.1 us -> 55.3 us  [local(): pl.pallas_call(kernel, out_shape=pltpu.VMEM((256, HALF), BF16), in_specs=...]
where the time goes in v8:
time: 56.2 us; the launch traced here: 56 us
  Pallas kernels  55.3 us (98%)
  local copies, waits for them, and re-layouts  0.71 us (1%)
    pallas_call x1, Pallas kernels, local(): pl.pallas_call(kernel, out_shape=pltpu.VMEM((256, HALF), BF16), in_specs=...  55.3 us

profile of v8, /device:TPU:1, one launch (start us, length us, event | category | flops | bytes accessed | tf_op | source)
XLA Modules:
  0.0 56.0 jit_solution(10136898428717161041)
XLA Ops:
  0.0 55.3 %shard_map.118 = bf16[256,512]{1,0:T(8,128)(2,1)S(1)} custom-call(bf16[256,512]{1,0:T(8,128)(2,1)} %bitcast.12, f32[1,1024]{1,0:T(1,128)} %bitcast.16, bf16[32,1280]{1,0:T(8,128)(2,1)} %gate1.1, bf16[32,1280]{1,0:T(8,128)(2,1)} %up1.1, bf16[32,1280]{1,0:T(8,128)(2,1)} %bitcast.13, f32[1,512]{1,0:T(1,128)} %bitcast.18, bf16[16,256]{1,0:T(8,128)(2,1)} %bitcast.15, ...), custom_call_target="tpu_custom_call" | custom-call | tf_op jit(solution)/shard_map/pallas_call | solution.py:673
  55.3 0.7 %copy.14 = bf16[1,256,512]{2,1,0:T(8,128)(2,1)} copy(bf16[1,256,512]{2,1,0:T(8,128)(2,1)S(1)} %bitcast.11) | data formatting | bytes 524288

commit v9 on v8

--- a/solution.py
+++ b/solution.py
@@ -14,8 +14,8 @@
 ROWS = 128
 UNIT = 640
 DIRECT = False
-N_SEND = 35
-N_RECV = 90
+N_SEND = 23
+N_RECV = 84
 N_LOCAL = 10
 
 
@@ -82,9 +82,9 @@
 
 
 class Stream:
-    def __init__(self, net, unit, tag, direct, piece, group, size, many, first, second, sibling):
+    def __init__(self, net, unit, tag, direct, piece, group, size, size_all, first, second, sibling):
         self.net, self.unit, self.tag, self.direct = net, unit, (unit, tag), direct
-        self.piece, self.group, self.size, self.many = piece, group, size, many
+        self.piece, self.group, self.size, self.size_all = piece, group, size, size_all
         self.a, self.ap, self.am, self.ao, self.to_ap, self.to_am, self.to_ao = first
         self.b, self.bp, self.bm, self.bo, self.to_bp, self.to_bm, self.to_bo = second
         self.sibling = sibling
@@ -94,15 +94,15 @@
         self.net.send(
             (self.tag, what),
             lambda: (self.piece(a, b), self.piece(a, b), device),
-            batch=(self.unit, kind),
-            total=lambda: self.size(count * self.many),
+            batch=kind,
+            total=lambda: self.size_all(count),
         )
 
     def recv(self, what, a, b):
         self.net.recv((self.tag, what), self.piece(a, b))
 
     def both(self, k, a):
-        late_m, late_p = ("2m23" if k >= 2 else f"2m{k}"), ("2p01" if k < 2 else f"2p{k}")
+        late_m, late_p = ("2x" if k >= 2 else f"2m{k}"), ("2x" if k < 2 else f"2p{k}")
         self.send(late_m, a, self.b, self.to_bp, "both", 8)
         self.send(late_p, a, self.b, self.to_bm, "both", 8)
 
@@ -110,8 +110,8 @@
         self.net.send(
             (self.unit, "d"),
             lambda: (self.group(b), self.group(b), self.sibling),
-            batch=(self.unit, "hand"),
-            total=lambda: self.size(16 * self.many),
+            batch="hand",
+            total=lambda: self.size_all(16),
         )
 
     def one(self):
@@ -148,9 +148,8 @@
     def four(self):
         self.recv("2p3", self.ao, self.bp)
         self.send("2o", self.ao, self.bp, self.to_bm, "on", 4)
-        self.net.recv((self.tag, "2p01"), self.size(2))
+        self.net.recv((self.tag, "2x"), self.size(4))
         self.hand(self.bp)
-        self.net.recv((self.tag, "2m23"), self.size(2))
         self.hand(self.bm)
 
     def five(self):
@@ -286,8 +285,8 @@
                         dev(z_, y, x, o),
                     ),
                     cond=taker,
-                    batch=("z", u),
-                    total=lambda: w.at[u, :, 0, 0, 0],
+                    batch="z",
+                    total=lambda: w.at[:, :, 0, 0, 0],
                 )
 
     def own(u):
@@ -306,12 +305,15 @@
     two, top, low = pl.ds(0, 2), pl.ds(0, 16), pl.ds(16, 16)
 
     def size_w(k):
+        return {2: w.at[0, :, 0, two, 0, top], 4: w.at[0, :, 0, :, 0, top]}[k]
+
+    def size_all(k):
         return {
-            2: w.at[0, :, 0, two, 0, top],
-            4: w.at[0, :, 0, :, 0, top],
-            8: w.at[0, :, 0, two, :, top],
-            16: w.at[0, :, 0, :, :, top],
-            32: w.at[0, :, 0],
+            1: w.at[:, :, 0, two, 0, top],
+            2: w.at[:, :, 0, :, 0, top],
+            4: w.at[:, :, 0, two, :, top],
+            8: w.at[:, :, 0, :, :, top],
+            16: w.at[:, :, 0],
         }[k]
 
     def stream_a(u):
@@ -319,7 +321,7 @@
             net, u, "a", DIRECT and u == 0,
             lambda a, b: w.at[u, :, c, b, a, top, :],
             lambda b: w.at[u, :, c, b, :, top, :],
-            size_w, 2, in_x, in_y, sibling,
+            size_w, size_all, in_x, in_y, sibling,
         )
 
     def stream_b(u):
@@ -327,7 +329,7 @@
             net, u, "b", DIRECT and u == 0,
             lambda a, b: w.at[u, :, c, a, b, low, :],
             lambda b: w.at[u, :, c, :, b, low, :],
-            size_w, 2, in_y, in_x, sibling,
+            size_w, size_all, in_y, in_x, sibling,
         )
 
     sa = [stream_a(u) for u in range(3)]

time: 56.2 us -> 56 us (level)
  no operation moved by 1% of the time
where the time goes in v9:
time: 56 us; the launch traced here: 55.9 us
  Pallas kernels  55.1 us (98%)
  local copies, waits for them, and re-layouts  0.71 us (1%)
    pallas_call x1, Pallas kernels, local(): pl.pallas_call(kernel, out_shape=pltpu.VMEM((256, HALF), BF16), in_specs=...  55.1 us

profile of v9, /device:TPU:1, one launch (start us, length us, event | category | flops | bytes accessed | tf_op | source)
XLA Modules:
  0.0 55.9 jit_solution(12745132662896061096)
XLA Ops:
  0.0 55.1 %shard_map.118 = bf16[256,512]{1,0:T(8,128)(2,1)S(1)} custom-call(bf16[256,512]{1,0:T(8,128)(2,1)} %bitcast.12, f32[1,1024]{1,0:T(1,128)} %bitcast.16, bf16[32,1280]{1,0:T(8,128)(2,1)} %gate1.1, bf16[32,1280]{1,0:T(8,128)(2,1)} %up1.1, bf16[32,1280]{1,0:T(8,128)(2,1)} %bitcast.13, f32[1,512]{1,0:T(1,128)} %bitcast.18, bf16[16,256]{1,0:T(8,128)(2,1)} %bitcast.15, ...), custom_call_target="tpu_custom_call" | custom-call | tf_op jit(solution)/shard_map/pallas_call | solution.py:675
  55.1 0.7 %copy.14 = bf16[1,256,512]{2,1,0:T(8,128)(2,1)} copy(bf16[1,256,512]{2,1,0:T(8,128)(2,1)S(1)} %bitcast.11) | data formatting | bytes 524288

commit v10 on v9

--- a/solution.py
+++ b/solution.py
@@ -15,7 +15,7 @@
 UNIT = 640
 DIRECT = False
 N_SEND = 23
-N_RECV = 84
+N_RECV = 81
 N_LOCAL = 10
 
 
@@ -465,9 +465,9 @@
                 f"r{k}", lambda k=k, z_=z_: (so.at[:, feats(k)], ra.at[k], dev(z_, y, x, c)), batch="r", total=lambda: so
             )
 
-    def pass_on(key, buf, k, half, z_):
+    def pass_on(buf, k, half, z_):
         net.send(
-            f"{key}{half}",
+            "q",
             lambda: (buf.at[:, feats(half)], rb.at[k, :, feats(half)], dev(z_, y, x, c)),
             batch="q", total=lambda: xt.at[two],
         )
@@ -479,8 +479,8 @@
         sp[:, HALF:] = sums[ROWS:, HALF:].astype(BF16)
         pm[...] = sums[:ROWS, HALF:]
         pp[...] = sums[ROWS:, :HALF]
-        pass_on("qm", sp, 0, 1, zp)
-        pass_on("qp", sm, 1, 0, zm)
+        pass_on(sp, 0, 1, zp)
+        pass_on(sm, 1, 0, zm)
 
     def first_own():
         gate_up(0, 0, ROWS, put1(0, ROWS))
@@ -489,10 +489,10 @@
     def first_pass_on():
         net.recv("r0", ra.at[0])
         sp[:, :HALF] = (pp[...] + ra[0].astype(F32)).astype(BF16)
-        pass_on("qm", sp, 0, 0, zp)
+        pass_on(sp, 0, 0, zp)
         net.recv("r1", ra.at[1])
         sm[:, HALF:] = (pm[...] + ra[1].astype(F32)).astype(BF16)
-        pass_on("qp", sm, 1, 1, zm)
+        pass_on(sm, 1, 1, zm)
 
     def pool_maps():
         spool.last(pw.at[:, o])
@@ -504,8 +504,7 @@
         return jnp.concatenate([mg[k, 0], mg[k, 1]], axis=1)
 
     def first_sum():
-        for key, k, half in (("qm", 0, 1), ("qp", 1, 0), ("qm", 0, 0), ("qp", 1, 1)):
-            net.recv(f"{key}{half}", rb.at[k, :, feats(half)])
+        net.recv("q", rb)
         net.recv("mg", mg.at[:, o])
 
     def halo():

time: 56 us -> 56 us (level)
  no operation moved by 1% of the time
where the time goes in v10:
time: 56 us; the launch traced here: 55.8 us
  Pallas kernels  55.1 us (98%)
  local copies, waits for them, and re-layouts  0.71 us (1%)
    pallas_call x1, Pallas kernels, local(): pl.pallas_call(kernel, out_shape=pltpu.VMEM((256, HALF), BF16), in_specs=...  55.1 us

profile of v10, /device:TPU:1, one launch (start us, length us, event | category | flops | bytes accessed | tf_op | source)
XLA Modules:
  0.0 55.8 jit_solution(1486564099817147496)
XLA Ops:
  0.0 55.1 %shard_map.118 = bf16[256,512]{1,0:T(8,128)(2,1)S(1)} custom-call(bf16[256,512]{1,0:T(8,128)(2,1)} %bitcast.12, f32[1,1024]{1,0:T(1,128)} %bitcast.16, bf16[32,1280]{1,0:T(8,128)(2,1)} %gate1.1, bf16[32,1280]{1,0:T(8,128)(2,1)} %up1.1, bf16[32,1280]{1,0:T(8,128)(2,1)} %bitcast.13, f32[1,512]{1,0:T(1,128)} %bitcast.18, bf16[16,256]{1,0:T(8,128)(2,1)} %bitcast.15, ...), custom_call_target="tpu_custom_call" | custom-call | tf_op jit(solution)/shard_map/pallas_call | solution.py:674
  55.1 0.7 %copy.14 = bf16[1,256,512]{2,1,0:T(8,128)(2,1)} copy(bf16[1,256,512]{2,1,0:T(8,128)(2,1)S(1)} %bitcast.11) | data formatting | bytes 524288
